TPU v7x, 128 devices: a whole 4x4x4 slice. The times are simulated.
128 devices in a mesh: ep: 32 (over z, y, core), tp: 4 (over x).
Axes of the slice: x: 4, y: 4, z: 4, core: 2. Of those that a mesh axis runs over, the one named last changes fastest.
Arguments:
- value_in: bfloat16 [16384, 2048], P('ep', 'tp'), may hold values from -400 to 400
- gate_in: bfloat16 [16384, 2048], P('ep', 'tp'), may hold values from -8 to 8
- conv_taps: float32 [31, 2048], P(None, 'tp'), may hold values from -1 to 1
- conv_bias: float32 [2048], P('tp'), may hold values from -3 to 3
- ln_gain: float32 [2048], P('tp'), may hold values from 0.1 to 1.9
- ln_bias: float32 [2048], P('tp'), may hold values from -3 to 3
- out_proj: bfloat16 [2048, 4096], P('tp'), may hold values from -0.125 to 0.125
- tokens_b: bfloat16 [16384, 4096], P('ep'), may hold values from -6 to 6
- norm_gain: float32 [4096], replicated, may hold values from 0.1 to 1.9
- routes: int32 [16384, 2], P(('ep', 'tp')), may hold values from 0 to 31, all different within a row; in each aligned block of 128 rows (0 to 127, 128 to 255, ...) at most 12 rows name the same one
- route_weights: float32 [16384, 2], P(('ep', 'tp')), may hold values from 0.2 to 1.5
- expert_gate: bfloat16 [32, 4096, 1024], P('ep', None, 'tp'), may hold values from -0.09375 to 0.09375
- expert_up: bfloat16 [32, 4096, 1024], P('ep', None, 'tp'), may hold values from -0.09375 to 0.09375
- expert_down: bfloat16 [32, 1024, 4096], P('ep', 'tp'), may hold values from -0.1875 to 0.1875
- shared_gate: bfloat16 [4096, 1024], P(None, 'tp'), may hold values from -0.09375 to 0.09375
- shared_up: bfloat16 [4096, 1024], P(None, 'tp'), may hold values from -0.09375 to 0.09375
- shared_down: bfloat16 [1024, 4096], P('tp'), may hold values from -0.1875 to 0.1875
Outputs:
- mixer_out: bfloat16 [16384, 4096], P(('ep', 'tp'))
- experts_out: bfloat16 [16384, 4096], P(('ep', 'tp'))
Inputs may be any that keep to these rules, and one draw needn't show every extreme that they name: `routes`: each row names 2 different experts. In each aligned block of 128 rows (the rows of one device) no expert is named by more than 12 rows, and in some blocks an expert is named by exactly 12 rows.
All inputs are finite; a program needn't handle non-finite values.
Results may differ from a plain program's by a relative error of at most 0.012.
Values may be sent and summed in bfloat16 or wider, within the bound.
A program may use at most 128 MiB of HBM per device.

v0:
```python
import jax
import jax.numpy as jnp
from jax import lax
from jax.sharding import PartitionSpec as P

EPSILON = 1e-06


def shifted(x, axis, by):
    devices = lax.axis_size(axis)
    pairs = [(i, i + by) for i in range(devices) if 0 <= i + by < devices]
    return lax.ppermute(x, axis, pairs)


def from_everyone(x, axis):
    devices = lax.axis_size(axis)
    return lax.all_to_all(jnp.broadcast_to(x[None], (devices, *x.shape)), axis, 0, 0, tiled=True)


def taken_together(x, axis):
    everything = from_everyone(x, axis)
    return jnp.sum(everything, axis=0)


def packed_total(arrays, axis):
    ends = [0]
    for a in arrays:
        ends.append(ends[-1] + a.size)
    running = taken_together(jnp.concatenate([a.ravel() for a in arrays]), axis)
    return tuple((running[b:e].reshape(a.shape) for a, b, e in zip(arrays, ends, ends[1:])))


def joined_along(blocks, dim):
    blocks = jnp.moveaxis(blocks, 0, dim)
    dims = blocks.shape
    return blocks.reshape(*dims[:dim], dims[dim] * dims[dim + 1], *dims[dim + 2 :])


def gathered_copies(x, axis, dim):
    return joined_along(from_everyone(x, axis), dim)


def slot_table(route_ids, expert_count):
    chosen = route_ids.reshape(-1)
    onehot = (chosen[:, None] == jnp.arange(expert_count, dtype=jnp.int32)[None, :]).astype(
        jnp.int32
    )
    earlier = jnp.cumsum(onehot, axis=0) - onehot
    return (chosen, jnp.sum(earlier * onehot, axis=1))


def gated_hidden(rows_in, weight_gate, weight_up):
    row_shape = rows_in.shape
    matrix = rows_in.reshape(-1, row_shape[-1])
    hidden = (
        jax.nn.silu(jnp.dot(matrix, weight_gate, preferred_element_type=jnp.float32))
        * jnp.dot(matrix, weight_up, preferred_element_type=jnp.float32)
    ).astype(jnp.bfloat16)
    return hidden.reshape(row_shape[:-1] + (weight_gate.shape[1],))


def project_down(hidden, weight):
    row_shape = hidden.shape
    product = jnp.dot(hidden.reshape(-1, row_shape[-1]), weight, preferred_element_type=jnp.float32)
    return product.reshape(row_shape[:-1] + (weight.shape[1],))


def per_device(
    value_in,
    gate_in,
    conv_taps,
    conv_bias,
    ln_gain,
    ln_bias,
    out_proj,
    tokens_b,
    norm_gain,
    routes,
    route_weights,
    expert_gate,
    expert_up,
    expert_down,
    shared_gate,
    shared_up,
    shared_down,
):
    tp_count = lax.axis_size("tp")
    ep_count = lax.axis_size("ep")
    gated = (value_in.astype(jnp.float32) * jax.nn.sigmoid(gate_in.astype(jnp.float32))).astype(
        jnp.bfloat16
    )
    rim_rows = conv_taps.shape[0] - 1
    length = gated.shape[0]
    before = shifted(gated[length - rim_rows :], "ep", 1)
    padded = jnp.concatenate([before, gated], axis=0).astype(jnp.float32)
    filtered = jnp.zeros(gated.shape, jnp.float32) + conv_bias[None, :]
    for tap_index in range(rim_rows + 1):
        filtered = filtered + conv_taps[tap_index][None, :] * padded[tap_index : tap_index + length]
    row_sum, squares = packed_total(
        (jnp.sum(filtered, axis=1), jnp.sum(filtered * filtered, axis=1)), "tp"
    )
    channel_count = filtered.shape[1] * tp_count
    average = row_sum / channel_count
    variance = squares / channel_count - average * average
    normed_a = (filtered - average[:, None]) * lax.rsqrt(
        variance[:, None] + EPSILON
    ) * ln_gain + ln_bias
    activated = jax.nn.silu(normed_a).astype(jnp.bfloat16)
    features = tokens_b.astype(jnp.float32)
    normed_b = (
        features
        * lax.rsqrt(jnp.mean(features * features, axis=1, keepdims=True) + EPSILON)
        * norm_gain
    ).astype(jnp.bfloat16)
    rows_own, top_count = routes.shape
    model_width = normed_b.shape[1]
    own_rows = lax.dynamic_slice_in_dim(normed_b, lax.axis_index("tp") * rows_own, rows_own, 0)
    capacity = max(2, 3 * rows_own * top_count // (2 * ep_count))
    chosen, places = slot_table(routes, ep_count)
    source = jnp.repeat(own_rows, top_count, axis=0)
    outbox = (
        jnp.zeros((ep_count, capacity, model_width), jnp.bfloat16).at[chosen, places].set(source)
    )
    gate_local = expert_gate[0]
    up_local = expert_up[0]
    down_local = expert_down[0]
    arrived = lax.all_to_all(outbox, "ep", split_axis=0, concat_axis=0, tiled=True)
    hidden_routed = gated_hidden(gathered_copies(arrived[None], "tp", 0), gate_local, up_local)
    hidden_routed = hidden_routed.reshape(tp_count, ep_count * capacity, -1)
    hidden_shared = gated_hidden(normed_b, shared_gate, shared_up).reshape(tp_count, rows_own, -1)
    mixer_rows = lax.psum_scatter(
        jnp.dot(activated, out_proj, preferred_element_type=jnp.float32).astype(jnp.bfloat16),
        "tp",
        scatter_dimension=0,
        tiled=True,
    )
    summed = lax.psum_scatter(
        jnp.concatenate(
            [project_down(hidden_routed, down_local), project_down(hidden_shared, shared_down)],
            axis=1,
        ).astype(jnp.bfloat16),
        "tp",
        scatter_dimension=0,
        tiled=True,
    ).astype(jnp.float32)[0]
    summed = summed.astype(jnp.bfloat16)
    routed_rows = summed[: ep_count * capacity].reshape(ep_count, capacity, model_width)
    shared_rows = summed[ep_count * capacity :]
    returned = lax.all_to_all(routed_rows, "ep", split_axis=0, concat_axis=0, tiled=True)
    picked = returned[chosen, places].astype(jnp.float32) * route_weights.reshape(-1)[:, None]
    experts_out = (
        shared_rows.astype(jnp.float32)
        + jnp.sum(picked.reshape(rows_own, top_count, model_width), axis=1)
    ).astype(jnp.bfloat16)
    return (mixer_rows, experts_out)


def solution(mesh):
    return jax.shard_map(
        per_device,
        mesh=mesh,
        in_specs=(
            P("ep", "tp"),
            P("ep", "tp"),
            P(None, "tp"),
            P("tp"),
            P("tp"),
            P("tp"),
            P("tp", None),
            P("ep", None),
            P(),
            P(("ep", "tp"), None),
            P(("ep", "tp"), None),
            P("ep", None, "tp"),
            P("ep", None, "tp"),
            P("ep", "tp", None),
            P(None, "tp"),
            P(None, "tp"),
            P("tp", None),
        ),
        out_specs=(P(("ep", "tp"), None), P(("ep", "tp"), None)),
        check_vma=False,
    )
```

profile of v0, /device:TPU:1, one launch (start us, length us, event | category | flops | bytes accessed | tf_op | source)
XLA Modules:
  0.0 626.3 jit_solution(1816978433081984892)
XLA Ops:
  21.9 4.1 reshape.133
  28.2 66.5 %scatter_fusion = bf16[32,12,4096]{2,0,1:T(8,128)(2,1)} fusion(bf16[32,12,4096]{2,0,1:T(8,128)(2,1)} %broadcast_in_dim.9, s32[256]{0:T(256)S(1)} %bitcast.82, bf16[256,4096]{1,0:T(8,128)(2,1)} %reshape.133), kind=kCustom, calls=%fused_computation.1 | custom fusion | bytes 6293504 | tf_op jit(solution)/shard_map/scatter | solution.py:122
  98.4 60.2 %all_to_all.21 = bf16[32,12,4096]{2,1,0:T(8,128)(2,1)S(1)} all-to-all(bf16[32,12,4096]{2,1,0:T(8,128)(2,1)S(1)} %copy.52), channel_id=1, replica_groups=mesh['ep'=32,'tp'=4] {'ep'}, dimensions={0} | all-to-all | bytes 6291456 | tf_op jit(solution)/shard_map/all_to_all | solution.py:127
  162.0 8.1 %broadcast_in_dim.11 = bf16[4,1,32,12,4096]{4,2,3,1,0:T(8,128)(2,1)} broadcast(bf16[32,12,4096]{2,0,1:T(8,128)(2,1)} %copy.53), dimensions={2,3,4} | broadcast | bytes 15728640 | tf_op jit(solution)/shard_map/broadcast_in_dim | solution.py:17
  170.1 6.7 %all-to-all-start.2 = ((bf16[4,1,32,12,4096]{4,2,3,1,0:T(8,128)(2,1)}), bf16[4,1,32,12,4096]{4,2,3,1,0:T(8,128)(2,1)}, u32[]{:S(2)}, u32[]{:S(2)}) async-start(bf16[4,1,32,12,4096]{4,2,3,1,0:T(8,128)(2,1)} %broadcast_in_dim.11), calls=%async_computation.3 | async-start | bytes 25165824 | tf_op jit(solution)/shard_map/all_to_all | solution.py:17
  176.8 4.1 fusion.64
  180.9 9.9 %convolution_convert_fusion.1 = bf16[512,4096]{1,0:T(8,128)(2,1)} fusion(bf16[256,4096]{1,0:T(8,128)(2,1)} %param.33, bf16[512,4096]{1,0:T(8,128)(2,1)} %copy-done.3, bf16[4096,256]{1,0:T(8,128)(2,1)} %param.32, f32[512,256]{1,0:T(8,128)S(1)} %fusion.64), kind=kOutput, calls=%fused_computation.9 | convolution fusion | flops 2150367232 | bytes 13107200 | tf_op jit(solution)/shard_map/dot_general | solution.py:64
  190.8 124.4 %all-to-all-done.2 = bf16[4,1,32,12,4096]{4,2,3,1,0:T(8,128)(2,1)} async-done(((bf16[4,1,32,12,4096]{4,2,3,1,0:T(8,128)(2,1)}), bf16[4,1,32,12,4096]{4,2,3,1,0:T(8,128)(2,1)}, u32[]{:S(2)}, u32[]{:S(2)}) %all-to-all-start.2) | async-done | bytes 12582944 | tf_op jit(solution)/shard_map/all_to_all | solution.py:17
  315.2 13.8 %copy.54 = bf16[4,1,32,12,4096]{4,3,2,0,1:T(8,128)(2,1)} copy(bf16[4,1,32,12,4096]{4,2,3,1,0:T(8,128)(2,1)} %all-to-all-done.2) | data formatting | bytes 25165824 | tf_op jit(solution)/shard_map/all_to_all | solution.py:17
  329.0 18.2 %reshape_reshape.3 = bf16[1536,4096]{1,0:T(8,128)(2,1)} reshape(bf16[4,1,32,12,4096]{4,3,2,0,1:T(8,128)(2,1)} %copy.54) | data formatting | bytes 25165824 | tf_op jit(solution)/shard_map/reshape;reshape | solution.py:54
  347.2 7.7 %fusion.7 = f32[1536,256]{1,0:T(8,128)S(1)} fusion(bf16[1536,4096]{1,0:T(8,128)(2,1)} %reshape_reshape.3, bf16[1,4096,256]{2,1,0:T(8,128)(2,1)} %param.28), kind=kOutput, calls=%fused_computation.18 | convolution fusion | flops 3221225472 | bytes 16252928 | tf_op jit(solution)/shard_map/dot_general | solution.py:56
  360.4 6.4 %convolution_convert_fusion = bf16[4,384,4096]{2,1,0:T(8,128)(2,1)} fusion(bf16[4,384,256]{2,1,0:T(8,128)(2,1)S(1)} %bitcast.84, bf16[1,256,4096]{2,1,0:T(8,128)(2,1)S(1)} %copy-done), kind=kOutput, calls=%fused_computation.5 | convolution fusion | flops 3227516928 | bytes 15466496 | tf_op jit(solution)/shard_map/dot_general | solution.py:64
  366.9 12.3 %pad_maximum_fusion = bf16[4,512,4096]{2,1,0:T(8,128)(2,1)} fusion(bf16[4,128,4096]{2,1,0:T(8,128)(2,1)S(1)} %bitcast.83, bf16[4,384,4096]{2,1,0:T(8,128)(2,1)} %convolution_convert_fusion), kind=kLoop, calls=%fused_computation.2 | loop fusion | flops 33554432 | bytes 33554432 | tf_op jit(solution)/shard_map/concatenate | solution.py:138
  385.5 5.0 fusion.59
  390.5 7.1 %all_to_all.22 = f32[4,1,1024]{2,1,0:T(1,128)S(1)} all-to-all(f32[4,1,1024]{2,1,0:T(1,128)S(1)} %broadcast_in_dim.8), channel_id=1, replica_groups=mesh['ep'=32,'tp'=4] {'tp'}, dimensions={0} | all-to-all | bytes 32768 | tf_op jit(solution)/shard_map/all_to_all | solution.py:17
  397.6 6.7 %convolution_convert_fusion.2 = bf16[512,4096]{1,0:T(8,128)(2,1)} fusion(bf16[512,4096]{1,0:T(8,128)(2,1)} %param.23, f32[512,512]{1,0:T(8,128)S(1)} %get-tuple-element.6, f32[512]{0:T(512)S(1)} %copy-done.13, f32[512]{0:T(512)S(1)} %copy-done.14, f32[512]{0:T(512)S(1)} %get-tuple-element.39, f32[512]{0:T(512)S(1)} %get-tuple-element.38), kind=kOutput, calls=%fused_computation.10 | convolution fusion | flops 2151940096 | bytes 9445376 | tf_op jit(solution)/shard_map/dot_general | solution.py:132
  404.4 119.7 %reduce-scatter.5.cloned.1.call-done = bf16[1,512,4096]{2,1,0:T(8,128)(2,1)} async-done(((bf16[4,512,4096]{2,1,0:T(8,128)(2,1)}), bf16[1,512,4096]{2,1,0:T(8,128)(2,1)}) %reduce-scatter.5.cloned.1.call-update) | async-done | bytes 4194320 | tf_op jit(solution)/shard_map/reduce_scatter | solution.py:137
  528.0 5.5 reshape.122
  533.5 8.0 %all-to-all-start.3 = ((bf16[32,12,4096]{2,1,0:T(8,128)(2,1)}), bf16[32,12,4096]{2,1,0:T(8,128)(2,1)}, u32[]{:S(2)}, u32[]{:S(2)}) async-start(bf16[32,12,4096]{2,1,0:T(8,128)(2,1)} %reshape.122), calls=%async_computation.5 | async-start | bytes 8388608 | tf_op jit(solution)/shard_map/all_to_all | solution.py:149
  541.6 50.6 %all-to-all-done.3 = bf16[32,12,4096]{2,1,0:T(8,128)(2,1)} async-done(((bf16[32,12,4096]{2,1,0:T(8,128)(2,1)}), bf16[32,12,4096]{2,1,0:T(8,128)(2,1)}, u32[]{:S(2)}, u32[]{:S(2)}) %all-to-all-start.3) | async-done | bytes 3145760 | tf_op jit(solution)/shard_map/all_to_all | solution.py:149
  592.1 5.6 copy.55
  597.7 5.9 gather_fusion
  603.7 4.2 reshape.124
  607.9 8.9 %multiply_reduce_fusion = f32[128,4096]{1,0:T(8,128)S(1)} fusion(f32[128,2,4096]{2,1,0:T(2,128)} %reshape.124, f32[128,2]{1,0:T(8,128)S(1)} %copy.56), kind=kLoop, calls=%fused_computation.11 | loop fusion | flops 1572864 | bytes 6292480 | tf_op jit(solution)/shard_map/reduce_sum | solution.py:153
  (70 shorter events, 42.1 us)
Async XLA Ops:
  7.2 353.3 %copy-start = (bf16[1,256,4096]{2,1,0:T(8,128)(2,1)S(1)}, bf16[1,256,4096]{2,1,0:T(8,128)(2,1)}, u32[]{:S(2)}) copy-start(bf16[1,256,4096]{2,1,0:T(8,128)(2,1)} %param.30) | copy-start | bytes 6291460
  7.2 5.3 copy-start.8
  9.4 6.9 %copy-start.9 = (s32[32,3]{0,1:T(4,128)}, s32[32,3]{0,1:T(4,128)S(1)}, u32[]{:S(2)}) copy-start(s32[32,3]{0,1:T(4,128)S(1)} %reduce-window.9) | copy-start | bytes 1156
  16.3 2.0 copy-start.3
  18.4 7.6 %slice-start = ((s32[32,3]{0,1:T(4,128)}), s32[32,2]{0,1:T(2,128)S(1)}, s32[]{:S(2)}) async-start(s32[32,3]{0,1:T(4,128)} %copy-done.9), calls=%async_computation.8 | async-start | bytes 2048 | tf_op jit(solution)/shard_map/slice.1
  170.1 145.1 %all-to-all-start.2 = ((bf16[4,1,32,12,4096]{4,2,3,1,0:T(8,128)(2,1)}), bf16[4,1,32,12,4096]{4,2,3,1,0:T(8,128)(2,1)}, u32[]{:S(2)}, u32[]{:S(2)}) async-start(bf16[4,1,32,12,4096]{4,2,3,1,0:T(8,128)(2,1)} %broadcast_in_dim.11), calls=%async_computation.3 | async-start | bytes 25165824 | tf_op jit(solution)/shard_map/all_to_all | solution.py:17
  176.7 347.3 %reduce-scatter.5.cloned.1.call-start = ((), (), s32[]{:S(2)}) async-start(), calls=%async_computation.7 | async-start | bytes 20971520 | tf_op jit(solution)/shard_map/reduce_scatter | solution.py:137
  347.2 8.8 %copy-start.2 = (bf16[1536,4096]{1,0:T(8,128)(2,1)S(1)}, bf16[1536,4096]{1,0:T(8,128)(2,1)}, u32[]{:S(2)}) copy-start(bf16[1536,4096]{1,0:T(8,128)(2,1)} %reshape_reshape.3) | copy-start | bytes 37748740
  347.2 9.4 %copy-start.12 = (bf16[1,4096,256]{2,1,0:T(8,128)(2,1)S(1)}, bf16[1,4096,256]{2,1,0:T(8,128)(2,1)}, u32[]{:S(2)}) copy-start(bf16[1,4096,256]{2,1,0:T(8,128)(2,1)} %param.29) | copy-start | bytes 6291460
  360.4 6.4 %copy-start.4 = (bf16[512,4096]{1,0:T(8,128)(2,1)S(1)}, bf16[512,4096]{1,0:T(8,128)(2,1)}, u32[]{:S(2)}) copy-start(bf16[512,4096]{1,0:T(8,128)(2,1)} %convolution_convert_fusion.1) | copy-start | bytes 12582916
  379.2 1.0 copy-start.5
  379.2 1.2 copy-start.6
  379.2 5.0 copy-start.7
  379.3 6.2 copy-start.10
  379.3 239.9 %reduce-scatter.3.cloned.1.call-start = ((), (), s32[]{:S(2)}) async-start(), calls=%async_computation.6 | async-start | bytes 5242880 | tf_op jit(solution)/shard_map/reduce_scatter | solution.py:131
  380.7 4.5 collective-permute-start
  385.4 12.2 %copy-start.13 = (f32[512]{0:T(512)S(1)}, f32[512]{0:T(512)}, u32[]{:S(2)}) copy-start(f32[512]{0:T(512)} %param.22) | copy-start | bytes 6148
  385.4 12.2 %copy-start.14 = (f32[512]{0:T(512)S(1)}, f32[512]{0:T(512)}, u32[]{:S(2)}) copy-start(f32[512]{0:T(512)} %param.21) | copy-start | bytes 6148
  533.5 8.0 %copy-start.11 = (f32[128,2]{0,1:T(2,128)S(1)}, f32[128,2]{0,1:T(2,128)}, u32[]{:S(2)}) copy-start(f32[128,2]{0,1:T(2,128)} %param.27) | copy-start | bytes 3076
  533.5 58.7 %all-to-all-start.3 = ((bf16[32,12,4096]{2,1,0:T(8,128)(2,1)}), bf16[32,12,4096]{2,1,0:T(8,128)(2,1)}, u32[]{:S(2)}, u32[]{:S(2)}) async-start(bf16[32,12,4096]{2,1,0:T(8,128)(2,1)} %reshape.122), calls=%async_computation.5 | async-start | bytes 8388608 | tf_op jit(solution)/shard_map/all_to_all | solution.py:149
  607.8 11.3 %copy-start.1 = (bf16[1,256,4096]{2,1,0:T(8,128)(2,1)S(1)}, bf16[1,256,4096]{2,1,0:T(8,128)(2,1)}, u32[]{:S(2)}) copy-start(bf16[1,256,4096]{2,1,0:T(8,128)(2,1)} %param.30) | copy-start | bytes 6291460
Sparse Core Ops, SparseCore 0:
  379.4 144.6 reduce-scatter.4
  527.0 46.5 reduce-scatter.2
where the time goes:
time: 639 us; the launch traced here: 626 us
  waiting for transfers between devices  296 us (46%)
  local copies, waits for them, and re-layouts  155 us (24%)
  blocking collectives  67.3 us (11%)
  matrix products  38.8 us (6%)
  other arithmetic  36.8 us (6%)
  starting transfers between devices  18.2 us (3%)
  between operations  14.6 us (2%)
    all_to_all x1, waiting for transfers between devices, from_everyone(): lax.all_to_all(jnp.broadcast_to(x[None], (devices, *x.shape)), axis, 0, 0...  124 us
    reduce_scatter x1, waiting for transfers between devices, per_device(): lax.psum_scatter(jnp.concatenate([project_down(hidden_routed, down_local)...  120 us
    scatter x2, local copies, waits for them, and re-layouts, per_device(): jnp.zeros((ep_count, capacity, model_width), jnp.bfloat16)  70.2 us
    all_to_all x1, blocking collectives, per_device(): lax.all_to_all(outbox, 'ep', split_axis=0, concat_axis=0, tiled=True)  60.2 us
    all_to_all x1, waiting for transfers between devices, per_device(): lax.all_to_all(routed_rows, 'ep', split_axis=0, concat_axis=0, tiled=True)  50.6 us
    another operation x1, local copies, waits for them, and re-layouts, gated_hidden(): matrix = rows_in.reshape(-1, row_shape[-1])  18.2 us
    dot_general x2, matrix products, project_down(): jnp.dot(hidden.reshape(-1, row_shape[-1]), weight, preferred_element_type...  16.3 us
    all_to_all x1, local copies, waits for them, and re-layouts, from_everyone(): lax.all_to_all(jnp.broadcast_to(x[None], (devices, *x.shape)), axis, 0, 0...  13.8 us
  transfers between devices with their start and end apart: 5, of which 4 were waited for; matrix products, arithmetic and copies ran while one was open for 10% of the time, Pallas kernels for 0%

commit v1 on v0

v1 whole, which is shorter than its diff:
```python
import functools

import jax
import jax.numpy as jnp
from jax import lax
from jax.experimental import pallas as pl
from jax.experimental.pallas import tpu as pltpu
from jax.sharding import PartitionSpec as P

EPSILON = 1e-06
MESH = pl.DeviceIdType.MESH
CAP = 12
BF = jnp.bfloat16
F32 = jnp.float32


def expert_kernel(
    outbox,
    gate,
    up,
    down,
    ret,
    inbox,
    hid,
    wdn,
    outs,
    acc,
    sem_local,
    ds,
    dr,
    fs,
    fr,
    hs,
    hr,
    ws,
    wr,
    rs,
    rr,
):
    me = lax.axis_index("ep")
    t = lax.axis_index("tp")
    z, y, c = me // 8, (me // 2) % 4, me % 2
    p = t % 2
    rows = outbox.shape[1]
    half = outbox.shape[2]
    group = 8 * rows
    units = gate.shape[1]
    width = wdn.shape[1]
    depth = gate.shape[0]

    def offset(i):
        dy = (i // 2) % 4
        return (i // 8 + dy) % 4, dy, i % 2

    def ahead(i):
        dz, dy, dc = offset(i)
        return ((z + dz) % 4) * 8 + ((y + dy) % 4) * 2 + (c + dc) % 2

    def behind(i):
        dz, dy, dc = offset(i)
        return ((z + 4 - dz) % 4) * 8 + ((y + 4 - dy) % 4) * 2 + (c + dc) % 2

    def column(j):
        return (t + j) % 4

    def features(q, size):
        return pl.ds(pl.multiple_of(q * size, size), size)

    barrier = pltpu.get_barrier_semaphore()
    for i in range(1, 32):
        pl.semaphore_signal(barrier, inc=1, device_id={"ep": ahead(i)}, device_id_type=MESH)
    for j in range(1, 4):
        pl.semaphore_signal(barrier, inc=1, device_id={"tp": column(j)}, device_id_type=MESH)
    pl.semaphore_wait(barrier, 34)

    def weight_copy(j):
        return pltpu.make_async_remote_copy(
            src_ref=down.at[:, features(column(j), width)],
            dst_ref=wdn.at[features(t, units), :],
            send_sem=ws.at[j],
            recv_sem=wr.at[j],
            device_id={"tp": column(j)},
            device_id_type=MESH,
        )

    own_weight = pltpu.make_async_copy(
        down.at[:, features(t, width)], wdn.at[features(t, units), :], sem_local.at[0]
    )
    own_rows = pltpu.make_async_copy(
        outbox.at[me], inbox.at[pl.ds(0, rows), features(p, half)], sem_local.at[1]
    )

    def dispatch(i):
        return pltpu.make_async_remote_copy(
            src_ref=outbox.at[ahead(i)],
            dst_ref=inbox.at[pl.ds(i * rows, rows), features(p, half)],
            send_sem=ds.at[i],
            recv_sem=dr.at[i],
            device_id={"ep": ahead(i)},
            device_id_type=MESH,
        )

    def forward(i):
        place = inbox.at[pl.ds(i * rows, rows), features(p, half)]
        return pltpu.make_async_remote_copy(
            src_ref=place,
            dst_ref=place,
            send_sem=fs.at[i],
            recv_sem=fr.at[i],
            device_id={"tp": column(1 if i % 2 == 0 else 3)},
            device_id_type=MESH,
        )

    def hidden_copy(g, j):
        place = hid.at[pl.ds(g * group, group), features(t, units)]
        return pltpu.make_async_remote_copy(
            src_ref=place,
            dst_ref=place,
            send_sem=hs.at[g, j],
            recv_sem=hr.at[g, j],
            device_id={"tp": column(j)},
            device_id_type=MESH,
        )

    def give_back(i):
        return pltpu.make_async_remote_copy(
            src_ref=outs.at[pl.ds(i * rows, rows), :],
            dst_ref=ret.at[me],
            send_sem=rs.at[i],
            recv_sem=rr.at[i],
            device_id={"ep": behind(i)},
            device_id_type=MESH,
        )

    own_back = pltpu.make_async_copy(outs.at[pl.ds(0, rows), :], ret.at[me], sem_local.at[2])

    own_rows.start()
    for i in range(1, 32):
        dispatch(i).start()
    own_weight.start()
    for j in range(1, 4):
        weight_copy(j).start()

    def receive(g):
        for i in range(8 * g, 8 * g + 8):
            if i == 0:
                own_rows.wait()
            else:
                dispatch(i).wait_recv()
            forward(i).start()

    def hidden(g):
        for i in range(8 * g, 8 * g + 8):
            forward(i).wait_recv()
        span = pl.ds(g * group, group)
        acc[...] = jnp.zeros_like(acc)
        step = 1024

        def body(k, carry):
            ks = pl.ds(pl.multiple_of(k * step, step), step)
            x = inbox[span, ks]
            acc[:, 0:units] += jnp.dot(x, gate[ks, :], preferred_element_type=F32)
            acc[:, units : 2 * units] += jnp.dot(x, up[ks, :], preferred_element_type=F32)
            return carry

        lax.fori_loop(0, depth // step, body, 0)
        a = acc[:, 0:units]
        hid[span, features(t, units)] = (
            a * (1.0 / (1.0 + jnp.exp(-a))) * acc[:, units : 2 * units]
        ).astype(BF)
        for j in range(1, 4):
            hidden_copy(g, j).start()

    def project(g):
        for j in range(1, 4):
            hidden_copy(g, j).wait_recv()
        span = pl.ds(g * group, group)
        step = 256

        def body(k, carry):
            ks = pl.ds(pl.multiple_of(k * step, step), step)
            outs[span, ks] = jnp.dot(
                hid[span, :], wdn[:, ks], preferred_element_type=F32
            ).astype(BF)
            return carry

        lax.fori_loop(0, width // step, body, 0)
        for i in range(8 * g, 8 * g + 8):
            if i == 0:
                own_back.start()
            else:
                give_back(i).start()

    receive(0)
    receive(1)
    hidden(0)
    receive(2)
    hidden(1)
    own_weight.wait()
    for j in range(1, 4):
        weight_copy(j).wait()
    project(0)
    receive(3)
    hidden(2)
    project(1)
    hidden(3)
    project(2)
    project(3)

    for i in range(1, 32):
        dispatch(i).wait_send()
    for i in range(32):
        forward(i).wait_send()
    for g in range(4):
        for j in range(1, 4):
            hidden_copy(g, j).wait_send()
    own_back.wait()
    for i in range(1, 32):
        give_back(i).wait()


def routed_rows(outbox, gate, up, down):
    count, rows, half = outbox.shape
    depth, units = gate.shape
    width = down.shape[1] // 4
    total = count * rows
    dma = pltpu.SemaphoreType.DMA
    vmem = pl.BlockSpec(memory_space=pltpu.VMEM)
    hbm = pl.BlockSpec(memory_space=pl.ANY)
    return pl.pallas_call(
        expert_kernel,
        out_shape=jax.ShapeDtypeStruct((count, rows, width), BF),
        in_specs=[hbm, vmem, vmem, hbm],
        out_specs=hbm,
        scratch_shapes=[
            pltpu.VMEM((total, depth), BF),
            pltpu.VMEM((total, 4 * units), BF),
            pltpu.VMEM((4 * units, width), BF),
            pltpu.VMEM((total, width), BF),
            pltpu.VMEM((total // 4, 2 * units), F32),
            dma((3,)),
            dma((32,)),
            dma((32,)),
            dma((32,)),
            dma((32,)),
            dma((4, 4)),
            dma((4, 4)),
            dma((4,)),
            dma((4,)),
            dma((32,)),
            dma((32,)),
        ],
        compiler_params=pltpu.CompilerParams(
            collective_id=0, has_side_effects=True, vmem_limit_bytes=56 * 1024 * 1024
        ),
        cost_estimate=pl.CostEstimate(
            flops=150_000_000_000, bytes_accessed=32 * 1024 * 1024, transcendentals=0
        ),
    )(outbox, gate, up, down)


def shifted(x, axis, by):
    devices = lax.axis_size(axis)
    pairs = [(i, i + by) for i in range(devices) if 0 <= i + by < devices]
    return lax.ppermute(x, axis, pairs)


def tap_filter(value_in, gate_in, conv_taps, conv_bias):
    gated = (value_in.astype(F32) * jax.nn.sigmoid(gate_in.astype(F32))).astype(BF)
    rim = conv_taps.shape[0] - 1
    length = gated.shape[0]
    before = shifted(gated[length - rim :], "ep", 1)
    padded = jnp.concatenate([before, gated], axis=0).astype(F32)
    filtered = jnp.zeros(gated.shape, F32) + conv_bias[None, :]
    for tap in range(rim + 1):
        filtered = filtered + conv_taps[tap][None, :] * padded[tap : tap + length]
    return filtered


def per_device(
    value_in,
    gate_in,
    conv_taps,
    conv_bias,
    ln_gain,
    ln_bias,
    out_proj,
    tokens_b,
    norm_gain,
    routes,
    route_weights,
    expert_gate,
    expert_up,
    expert_down,
    shared_gate,
    shared_up,
    shared_down,
):
    tp_count = lax.axis_size("tp")
    ep_count = lax.axis_size("ep")
    t = lax.axis_index("tp")
    rows_own, top_count = routes.shape
    rows_all = rows_own * tp_count
    model_width = tokens_b.shape[1]

    tables = lax.all_gather(
        jnp.concatenate([routes.astype(F32), route_weights], axis=1), "tp", axis=0
    )
    chosen = tables[:, :, :top_count].astype(jnp.int32).reshape(tp_count, -1)
    weights = tables[:, :, top_count:].reshape(rows_all, top_count)
    onehot = (chosen[:, :, None] == jnp.arange(ep_count, dtype=jnp.int32)).astype(BF)
    pairs = chosen.shape[1]
    lower = (
        jnp.arange(pairs, dtype=jnp.int32)[:, None] > jnp.arange(pairs, dtype=jnp.int32)[None, :]
    ).astype(BF)
    earlier = jnp.einsum("ij,bje->bie", lower, onehot, preferred_element_type=F32)
    places = jnp.sum(earlier * onehot.astype(F32), axis=2).astype(jnp.int32)
    slots = (
        chosen * (tp_count * CAP)
        + jnp.arange(tp_count, dtype=jnp.int32)[:, None] * CAP
        + places
    ).reshape(rows_all, top_count)
    slot_count = ep_count * tp_count * CAP

    features = tokens_b.astype(F32)
    normed_b = (
        features
        * lax.rsqrt(jnp.mean(features * features, axis=1, keepdims=True) + EPSILON)
        * norm_gain
    ).astype(BF)
    half = model_width // 2
    part = lax.dynamic_slice_in_dim(normed_b, (t % 2) * half, half, 1)
    ids = jnp.arange(slot_count, dtype=jnp.int32)
    select = (
        (ids[:, None] == slots[None, :, 0]) | (ids[:, None] == slots[None, :, 1])
    ).astype(BF)
    outbox = jnp.dot(select, part, preferred_element_type=F32).astype(BF)
    outbox = outbox.reshape(ep_count, tp_count * CAP, half)

    filtered = tap_filter(value_in, gate_in, conv_taps, conv_bias)
    sums = jnp.stack([jnp.sum(filtered, axis=1), jnp.sum(filtered * filtered, axis=1)])
    sums = jnp.sum(lax.all_gather(sums, "tp", axis=0), axis=0)
    channel_count = filtered.shape[1] * tp_count
    average = sums[0] / channel_count
    variance = sums[1] / channel_count - average * average
    normed_a = (filtered - average[:, None]) * lax.rsqrt(
        variance[:, None] + EPSILON
    ) * ln_gain + ln_bias
    activated = jax.nn.silu(normed_a).astype(BF)
    mixer_part = jnp.dot(activated, out_proj, preferred_element_type=F32).astype(BF)
    shared_hidden = (
        jax.nn.silu(jnp.dot(normed_b, shared_gate, preferred_element_type=F32))
        * jnp.dot(normed_b, shared_up, preferred_element_type=F32)
    ).astype(BF)
    shared_part = jnp.dot(shared_hidden, shared_down, preferred_element_type=F32).astype(BF)
    mixer_rows = lax.psum_scatter(mixer_part, "tp", scatter_dimension=0, tiled=True)
    shared_rows = lax.psum_scatter(shared_part, "tp", scatter_dimension=0, tiled=True)

    returned = routed_rows(outbox, expert_gate[0], expert_up[0], expert_down[0])
    returned = returned.reshape(slot_count, -1)
    spread = jnp.where(ids[None, :] == slots[:, 0:1], weights[:, 0:1], 0.0) + jnp.where(
        ids[None, :] == slots[:, 1:2], weights[:, 1:2], 0.0
    )
    high = spread.astype(BF)
    low = (spread - high.astype(F32)).astype(BF)
    combined = jnp.dot(high, returned, preferred_element_type=F32) + jnp.dot(
        low, returned, preferred_element_type=F32
    )
    quarters = lax.all_to_all(
        combined.astype(BF).reshape(tp_count, rows_own, -1), "tp", 0, 0, tiled=True
    )
    routed = jnp.moveaxis(quarters, 0, 1).reshape(rows_own, model_width)
    experts_out = (shared_rows.astype(F32) + routed.astype(F32)).astype(BF)
    return (mixer_rows, experts_out)


def solution(mesh):
    return jax.shard_map(
        per_device,
        mesh=mesh,
        in_specs=(
            P("ep", "tp"),
            P("ep", "tp"),
            P(None, "tp"),
            P("tp"),
            P("tp"),
            P("tp"),
            P("tp", None),
            P("ep", None),
            P(),
            P(("ep", "tp"), None),
            P(("ep", "tp"), None),
            P("ep", None, "tp"),
            P("ep", None, "tp"),
            P("ep", "tp", None),
            P(None, "tp"),
            P(None, "tp"),
            P("tp", None),
        ),
        out_specs=(P(("ep", "tp"), None), P(("ep", "tp"), None)),
        check_vma=False,
    )
```

time: 639 us -> 301 us (0.47); the launches traced: 626 us -> 298 us
  waiting for transfers between devices: 296 us -> 0.04 us
  Pallas kernels: 0 us -> 187 us
  local copies, waits for them, and re-layouts: 155 us -> 7.95 us
  blocking collectives: 67.3 us -> 36.9 us
  other arithmetic: 36.8 us -> 15.8 us
  starting transfers between devices: 18.2 us -> 4.66 us
  matrix products: 38.8 us -> 31.2 us
    pallas_call x0 -> x1, Pallas kernels: none -> 187 us  [routed_rows(): pl.pallas_call(expert_kernel, out_shape=jax.ShapeDtypeStruct((count, rows...]
    all_to_all x2 -> x0, waiting for transfers between devices: 175 us -> none  [the longest x1 124 us: from_everyone(): lax.all_to_all(jnp.broadcast_to(x[None], (devices, *x.shape)), axis, 0, 0...]
    reduce_scatter x2, waiting for transfers between devices: 120 us -> 0.01 us  [the longest x1 0.01 us: per_device(): lax.psum_scatter(shared_part, 'tp', scatter_dimension=0, tiled=True)]
    scatter x2 -> x0, local copies, waits for them, and re-layouts: 70.2 us -> none  [per_device(): jnp.zeros((ep_count, capacity, model_width), jnp.bfloat16)]
    all_to_all x2 -> x1, blocking collectives: 67.3 us -> 17.2 us  [per_device(): lax.all_to_all(combined.astype(BF).reshape(tp_count, rows_own, -1), 'tp',...]
    all_to_all x3 -> x0, local copies, waits for them, and re-layouts: 22.8 us -> none  [the longest x1 13.8 us: from_everyone(): lax.all_to_all(jnp.broadcast_to(x[None], (devices, *x.shape)), axis, 0, 0...]
    all_gather x0 -> x2, blocking collectives: none -> 19.7 us  [the longest x1 10.7 us: per_device(): sums = jnp.sum(lax.all_gather(sums, 'tp', axis=0), axis=0)]
    another operation x3 -> x0, local copies, waits for them, and re-layouts: 18.2 us -> none  [the longest x1 18.2 us: gated_hidden(): matrix = rows_in.reshape(-1, row_shape[-1])]
  transfers between devices with their start and end apart: 5 -> 3, of which waited for: 4 -> 0; matrix products, arithmetic and copies ran while one was open for 10% -> 12% of each run, Pallas kernels for 0% -> 63%
where the time goes in v1:
time: 301 us; the launch traced here: 298 us
  Pallas kernels  187 us (62%)
  blocking collectives  36.9 us (12%)
  matrix products  31.2 us (10%)
  other arithmetic  15.8 us (5%)
  between operations  14.5 us (5%)
  local copies, waits for them, and re-layouts  7.95 us (3%)
  starting transfers between devices  4.66 us (2%)
    pallas_call x1, Pallas kernels, routed_rows(): pl.pallas_call(expert_kernel, out_shape=jax.ShapeDtypeStruct((count, rows...  187 us
    all_to_all x1, blocking collectives, per_device(): lax.all_to_all(combined.astype(BF).reshape(tp_count, rows_own, -1), 'tp',...  17.2 us
    all_gather x1, blocking collectives, per_device(): sums = jnp.sum(lax.all_gather(sums, 'tp', axis=0), axis=0)  10.7 us
    dot_general x1, matrix products, per_device(): jnp.dot(shared_hidden, shared_down, preferred_element_type=F32).astype(BF)  9.36 us
    all_gather x1, blocking collectives, per_device(): lax.all_gather(jnp.concatenate([routes.astype(F32), route_weights], axis=...  9.01 us
    dot_general x1, matrix products, per_device(): outbox = jnp.dot(select, part, preferred_element_type=F32).astype(BF)  6.88 us
    dot_general x1, matrix products, per_device(): jnp.dot(activated, out_proj, preferred_element_type=F32).astype(BF)  6.86 us
  transfers between devices with their start and end apart: 3, of which 0 were waited for; matrix products, arithmetic and copies ran while one was open for 12% of the time, Pallas kernels for 63%

profile of v1, /device:TPU:1, one launch (start us, length us, event | category | flops | bytes accessed | tf_op | source)
XLA Modules:
  0.0 297.6 jit_solution(1527484800720007251)
XLA Ops:
  7.2 3.2 %fusion = f32[512]{0:T(512)S(1)} fusion(bf16[512,4096]{1,0:T(8,128)(2,1)} %param.24), kind=kLoop, calls=%fused_computation.2 | loop fusion | flops 6290944 | bytes 4196352 | tf_op jit(solution)/shard_map/reduce_sum | solution.py:328
  10.5 0.3 copy-done.1
  10.8 2.5 fusion.2
  13.4 2.1 copy-done.2
  15.4 1.3 fusion.76
  16.7 9.4 %convolution_convert_fusion.1 = bf16[512,4096]{1,0:T(8,128)(2,1)} fusion(bf16[256,4096]{1,0:T(8,128)(2,1)S(1)} %copy-done, bf16[512,4096]{1,0:T(8,128)(2,1)} %copy-done.2, bf16[4096,256]{1,0:T(8,128)(2,1)} %param.32, f32[512,256]{1,0:T(8,128)S(1)} %fusion.76), kind=kOutput, calls=%fused_computation.6 | convolution fusion | flops 2150367232 | bytes 13107200 | tf_op jit(solution)/shard_map/dot_general | solution.py:355
  26.2 0.9 copy-done.3
  27.1 1.3 multiply_convert_fusion.1
  28.5 4.6 %collective-permute-start = (bf16[30,512]{1,0:T(8,128)(2,1)S(1)}, bf16[30,512]{1,0:T(8,128)(2,1)S(1)}, u32[]{:S(2)}, u32[]{:S(2)}) collective-permute-start(bf16[30,512]{1,0:T(8,128)(2,1)S(1)} %slice.286), channel_id=1, source_target_pairs={{0,4},{4,8},{8,12},{12,16},{16,20},{20,24},{24,28},{28,32},{32,36}... | collective-permute-start | bytes 92168 | tf_op jit(solution)/shard_map/ppermute | solution.py:265
  33.1 9.0 %all-gather.1 = f32[512,4]{0,1:T(4,128)S(1)} all-gather(f32[128,4]{0,1:T(4,128)S(1)} %pad_maximum_fusion), channel_id=3, replica_groups=mesh['ep'=32,'tp'=4] {'tp'}, dimensions={0}, use_global_device_ids=true | all-gather | bytes 10240 | tf_op jit(solution)/shard_map/all_gather | solution.py:306
  42.2 0.6 slice_bitcast_fusion
  43.4 1.0 copy.30
  44.9 0.3 slice_reduce_fusion.1
  45.3 0.5 copy-done.7
  45.8 6.9 %convolution_convert_fusion = bf16[1536,2048]{1,0:T(8,128)(2,1)} fusion(bf16[512,4096]{1,0:T(8,128)(2,1)} %copy-done.2, s32[]{:T(128)S(6)} %select_n.20, s32[512]{0:T(512)S(1)} %get-tuple-element.5, s32[512]{0:T(512)S(1)} %get-tuple-element.4), kind=kOutput, calls=%fused_computation.5 | convolution fusion | flops 3226730496 | bytes 8392708 | tf_op jit(solution)/shard_map/dot_general | solution.py:337
  52.9 5.0 %fusion.71 = (f32[512]{0:T(512)S(1)}, f32[512]{0:T(512)S(1)}, f32[512,512]{1,0:T(8,128)S(1)}) fusion(f32[542,512]{1,0:T(8,128)S(1)} %maximum_convert_fusion, f32[512]{0:T(512)S(1)} %bitcast.113, f32[512]{0:T(512)S(1)} %bitcast.114, f32[512]{0:T(512)S(1)} %bitcast.85, f32[512]{0:T(512)S(1)} %bitcast.86, f32[512]{0:T(512)S(1)} %bitcast.87, ...), kind=kLoop, calls=%fused_computation.134 | loop fusion | flops 17038336 | bytes 33624064 | tf_op jit(solution)/shard_map/reduce_sum | solution.py:341
  57.9 10.7 %all-gather.2 = f32[4,2,512]{2,1,0:T(2,128)S(1)} all-gather(f32[1,2,512]{2,1,0:T(2,128)S(1)} %maximum_bitcast_fusion), channel_id=2, replica_groups=mesh['ep'=32,'tp'=4] {'tp'}, dimensions={0}, use_global_device_ids=true | all-gather | bytes 20480 | tf_op jit(solution)/shard_map/all_gather | solution.py:342
  68.7 6.9 %convolution_convert_fusion.2 = bf16[512,4096]{1,0:T(8,128)(2,1)} fusion(bf16[512,4096]{1,0:T(8,128)(2,1)} %param.23, f32[512,512]{1,0:T(8,128)S(1)} %get-tuple-element.6, f32[512]{0:T(512)S(1)} %copy-done.14, f32[512]{0:T(512)S(1)} %copy-done.15, f32[512]{0:T(512)S(1)} %add_rsqrt_fusion.1, f32[512]{0:T(512)S(1)} %bitcast.118), kind=kOutput, calls=%fused_computation.7 | convolution fusion | flops 2151940096 | bytes 9445376 | tf_op jit(solution)/shard_map/dot_general | solution.py:350
  75.6 186.6 %shard_map.176 = bf16[32,48,1024]{2,1,0:T(8,128)(2,1)} custom-call(bf16[32,48,2048]{2,1,0:T(8,128)(2,1)} %bitcast.127, bf16[4096,256]{1,0:T(8,128)(2,1)} %bitcast.124, bf16[4096,256]{1,0:T(8,128)(2,1)} %bitcast.125, bf16[256,4096]{1,0:T(8,128)(2,1)} %bitcast.126), custom_call_target="tpu_custom_call" | custom-call | flops 149999992832 | bytes 33554432 | tf_op jit(solution)/shard_map/pallas_call | solution.py:230
  262.3 4.1 %fusion.7 = f32[512,1024]{1,0:T(8,128)S(1)} fusion(bf16[1536,1024]{1,0:T(8,128)(2,1)} %bitcast.128, f32[512]{0:T(512)S(1)} %bitcast.122, s32[512]{0:T(512)S(1)} %copy-done.10, f32[512]{0:T(512)S(1)} %bitcast.120, s32[512]{0:T(512)S(1)} %copy-done.8), kind=kOutput, calls=%fused_computation.20 | convolution fusion | flops 1617690624 | bytes 5251072 | tf_op jit(solution)/shard_map/dot_general | solution.py:366
  266.4 2.4 add_convert_fusion.1
  268.9 17.2 %all_to_all.5 = bf16[4,128,1024]{2,1,0:T(8,128)(2,1)S(1)} all-to-all(bf16[4,128,1024]{2,1,0:T(8,128)(2,1)S(1)} %bitcast.81), channel_id=1, replica_groups=mesh['ep'=32,'tp'=4] {'tp'}, dimensions={0} | all-to-all | bytes 2097152 | tf_op jit(solution)/shard_map/all_to_all | solution.py:369
  286.3 1.5 copy.34
  287.8 3.0 %add_convert_fusion = bf16[128,4096]{1,0:T(8,128)(2,1)} fusion(f32[128,4096]{1,0:T(8,128)} %bitcast.80, bf16[128,4096]{1,0:T(8,128)(2,1)} %reduce-scatter.5.cloned.1.call-done), kind=kLoop, calls=%fused_computation.17 | loop fusion | flops 1572864 | bytes 4194304 | tf_op jit(solution)/shard_map/convert_element_type | solution.py:373
  (63 shorter events, 1.8 us)
Async XLA Ops:
  7.2 9.5 %copy-start = (bf16[256,4096]{1,0:T(8,128)(2,1)S(1)}, bf16[256,4096]{1,0:T(8,128)(2,1)}, u32[]{:S(2)}) copy-start(bf16[256,4096]{1,0:T(8,128)(2,1)} %param.33) | copy-start | bytes 6291460
  7.2 280.6 %reduce-scatter.5.cloned.1.call-start = ((), (), s32[]{:S(2)}) async-start(), calls=%async_computation.4 | async-start | bytes 5242880 | tf_op jit(solution)/shard_map/reduce_scatter | solution.py:357
  7.2 3.6 %copy-start.1 = (bf16[512,4096]{1,0:T(8,128)(2,1)S(1)}, bf16[512,4096]{1,0:T(8,128)(2,1)}, u32[]{:S(2)}) copy-start(bf16[512,4096]{1,0:T(8,128)(2,1)} %param.24) | copy-start | bytes 12582916
  10.8 4.6 %copy-start.13 = (bf16[4096,256]{1,0:T(8,128)(2,1)S(1)}, bf16[4096,256]{1,0:T(8,128)(2,1)}, u32[]{:S(2)}) copy-start(bf16[4096,256]{1,0:T(8,128)(2,1)} %param.31) | copy-start | bytes 6291460
  13.3 2.1 copy-start.2
  26.1 1.0 copy-start.3
  26.1 7.0 %copy-start.11 = (s32[128,2]{0,1:T(2,128)S(1)}, s32[128,2]{0,1:T(2,128)}, u32[]{:S(2)}) copy-start(s32[128,2]{0,1:T(2,128)} %param.26) | copy-start | bytes 3076
  26.1 7.0 %copy-start.12 = (f32[128,2]{0,1:T(2,128)S(1)}, f32[128,2]{0,1:T(2,128)}, u32[]{:S(2)}) copy-start(f32[128,2]{0,1:T(2,128)} %param.27) | copy-start | bytes 3076
  26.1 19.1 %copy-start.4 = (f32[31,512]{1,0:T(8,128)S(1)}, f32[31,512]{1,0:T(8,128)}, u32[]{:S(2)}) copy-start(f32[31,512]{1,0:T(8,128)} %param.19) | copy-start | bytes 190468
  26.1 264.7 %reduce-scatter.3.cloned.1.call-start = ((), (), s32[]{:S(2)}) async-start(), calls=%async_computation.3 | async-start | bytes 5242880 | tf_op jit(solution)/shard_map/reduce_scatter | solution.py:356
  28.5 24.2 %collective-permute-start = (bf16[30,512]{1,0:T(8,128)(2,1)S(1)}, bf16[30,512]{1,0:T(8,128)(2,1)S(1)}, u32[]{:S(2)}, u32[]{:S(2)}) collective-permute-start(bf16[30,512]{1,0:T(8,128)(2,1)S(1)} %slice.286), channel_id=1, source_target_pairs={{0,4},{4,8},{8,12},{12,16},{16,20},{20,24},{24,28},{28,32},{32,36}... | collective-permute-start | bytes 92168 | tf_op jit(solution)/shard_map/ppermute | solution.py:265
  45.2 0.6 copy-start.7
  45.2 0.6 copy-start.9
  45.8 7.1 %copy-start.6 = (f32[512]{0:T(512)S(1)}, f32[512]{0:T(512)}, u32[]{:S(2)}) copy-start(f32[512]{0:T(512)} %param.20) | copy-start | bytes 6148
  52.9 15.8 %copy-start.14 = (f32[512]{0:T(512)S(1)}, f32[512]{0:T(512)}, u32[]{:S(2)}) copy-start(f32[512]{0:T(512)} %param.22) | copy-start | bytes 6148
  52.9 15.8 %copy-start.15 = (f32[512]{0:T(512)S(1)}, f32[512]{0:T(512)}, u32[]{:S(2)}) copy-start(f32[512]{0:T(512)} %param.21) | copy-start | bytes 6148
  75.6 186.7 %copy-start.5 = (f32[1,2,4,128]{3,2,1,0:T(4,128)S(1)}, f32[1,2,4,128]{3,2,1,0:T(4,128)}, u32[]{:S(2)}) copy-start(f32[1,2,4,128]{3,2,1,0:T(4,128)} %get-tuple-element.38) | copy-start | bytes 12292
  75.6 186.7 %copy-start.8 = (s32[512]{0:T(512)S(1)}, s32[512]{0:T(512)}, u32[]{:S(2)}) copy-start(s32[512]{0:T(512)} %copy-done.7) | copy-start | bytes 6148
  75.6 186.7 %copy-start.10 = (s32[512]{0:T(512)S(1)}, s32[512]{0:T(512)}, u32[]{:S(2)}) copy-start(s32[512]{0:T(512)} %copy-done.9) | copy-start | bytes 6148
  262.3 4.1 %copy-start.16 = (bf16[32,48,1024]{2,1,0:T(8,128)(2,1)S(1)}, bf16[32,48,1024]{2,1,0:T(8,128)(2,1)}, u32[]{:S(2)}) copy-start(bf16[32,48,1024]{2,1,0:T(8,128)(2,1)} %shard_map.176) | copy-start | bytes 9437188
Sparse Core Ops, SparseCore 0:
  26.2 50.1 reduce-scatter.4
  79.4 91.8 reduce-scatter.2

commit v2 on v1

--- a/solution.py
+++ b/solution.py
@@ -16,16 +16,52 @@
 
 def expert_kernel(
     outbox,
-    gate,
-    up,
+    normed,
+    value_in,
+    gate_in,
+    taps,
+    conv_bias,
+    ln_gain,
+    ln_bias,
+    proj_in,
+    gate_hbm,
+    up_hbm,
     down,
+    sgate_hbm,
+    sup_hbm,
+    sdown_hbm,
     ret,
+    mixer_out,
+    shared_out,
     inbox,
     hid,
     wdn,
     outs,
     acc,
+    gate,
+    up,
+    padded,
+    filt,
+    act,
+    rim,
+    rim_out,
+    stats,
+    proj,
+    nb,
+    sgate,
+    sup,
+    sdown,
+    shid,
+    part,
+    first,
+    second,
     sem_local,
+    cs,
+    cr,
+    ss,
+    sr,
+    qs,
+    qr,
     ds,
     dr,
     fs,
@@ -66,6 +102,20 @@
     def features(q, size):
         return pl.ds(pl.multiple_of(q * size, size), size)
 
+    loads = [
+        pltpu.make_async_copy(a, b, sem_local.at[3 + n])
+        for n, (a, b) in enumerate(
+            [
+                (normed, nb),
+                (sgate_hbm, sgate),
+                (sup_hbm, sup),
+                (sdown_hbm, sdown),
+                (proj_in, proj),
+                (gate_hbm, gate),
+                (up_hbm, up),
+            ]
+        )
+    ]
     barrier = pltpu.get_barrier_semaphore()
     for i in range(1, 32):
         pl.semaphore_signal(barrier, inc=1, device_id={"ep": ahead(i)}, device_id_type=MESH)
@@ -140,6 +190,183 @@
     own_weight.start()
     for j in range(1, 4):
         weight_copy(j).start()
+    for load in loads:
+        load.start()
+
+    length, channels = value_in.shape
+    edge = rim.shape[0]
+    tap_count = taps.shape[0]
+    block = length // 4
+    wide = nb.shape[1]
+
+    rim_copy = pltpu.make_async_remote_copy(
+        src_ref=rim_out,
+        dst_ref=rim,
+        send_sem=cs.at[0],
+        recv_sem=cr.at[0],
+        device_id={"ep": (me + 1) % 32},
+        device_id_type=MESH,
+    )
+
+    def stats_copy(j):
+        return pltpu.make_async_remote_copy(
+            src_ref=stats.at[t],
+            dst_ref=stats.at[t],
+            send_sem=ss.at[j],
+            recv_sem=sr.at[j],
+            device_id={"tp": column(j)},
+            device_id_type=MESH,
+        )
+
+    def tiles(count, size, body):
+        def step(k, carry):
+            body(pl.ds(pl.multiple_of(k * size, size), size))
+            return carry
+
+        lax.fori_loop(0, count, step, 0)
+
+    def gated_tile(span):
+        g = gate_in[span, :].astype(F32)
+        v = value_in[span, :].astype(F32) * (1.0 / (1.0 + jnp.exp(-g)))
+        padded[pl.ds(pl.multiple_of(span.start + edge, edge), 64), :] = v.astype(BF).astype(F32)
+
+    tiles(length // 64, 64, gated_tile)
+    rim_out[...] = padded[length : length + edge, :].astype(BF)
+    rim_copy.start()
+
+    def shared_expert():
+        for load in loads[:4]:
+            load.wait()
+        acc[...] = jnp.zeros_like(acc)
+
+        def inner(ks):
+            x = nb[:, ks]
+            acc[:, 0:units] += jnp.dot(x, sgate[ks, :], preferred_element_type=F32)
+            acc[:, units : 2 * units] += jnp.dot(x, sup[ks, :], preferred_element_type=F32)
+
+        tiles(depth // 1024, 1024, inner)
+        a = acc[:, 0:units]
+        shid[...] = (a * (1.0 / (1.0 + jnp.exp(-a))) * acc[:, units : 2 * units]).astype(BF)
+
+        def outer(ks):
+            r = jnp.dot(shid[...], sdown[:, ks], preferred_element_type=F32).astype(BF)
+            for b in range(4):
+                part[b, block : 2 * block, ks] = r[b * block : (b + 1) * block, :]
+
+        tiles(wide // 512, 512, outer)
+
+    def convolve():
+        rim_copy.wait_recv()
+        padded[0:edge, :] = jnp.where(me == 0, 0.0, rim[...].astype(F32))
+
+        def strip(k, carry):
+            for q in range(channels // 128):
+                cols = slice(128 * q, 128 * q + 128)
+                window = padded[pl.ds(pl.multiple_of(k * 64, 64), 64 + edge), cols]
+                total = jnp.zeros((64, 128), F32) + conv_bias[:, cols]
+                for rest in range(8):
+                    turned = window[rest : rest + 56 + edge, :] if rest else window
+                    for tap in range(tap_count):
+                        at = edge + 1 - tap_count + tap
+                        if at % 8 == rest:
+                            base = at - rest
+                            total = total + taps[tap : tap + 1, cols] * turned[base : base + 64, :]
+                filt[pl.ds(pl.multiple_of(k * 64, 64), 64), cols] = total
+            return carry
+
+        lax.fori_loop(0, length // 64, strip, 0)
+        lane = lax.broadcasted_iota(jnp.int32, (128, 128), 1)
+        for b in range(length // 128):
+            rs_ = slice(128 * b, 128 * b + 128)
+            f = filt[rs_, :]
+            both = jnp.where(
+                lane == 0,
+                jnp.sum(f, axis=1, keepdims=True),
+                jnp.where(lane == 1, jnp.sum(f * f, axis=1, keepdims=True), 0.0),
+            )
+            stats[t, :, rs_] = both.T[0:8, :]
+        for j in range(1, 4):
+            stats_copy(j).start()
+
+    def activate():
+        for j in range(1, 4):
+            stats_copy(j).wait_recv()
+        whole = 4.0 * channels
+        for b in range(length // 128):
+            rs_ = slice(128 * b, 128 * b + 128)
+            total = (stats[0, :, rs_] + stats[1, :, rs_]) + (stats[2, :, rs_] + stats[3, :, rs_])
+            turned = jnp.concatenate([total, jnp.zeros((120, 128), F32)], axis=0).T
+            average = turned[:, 0:1] / whole
+            variance = turned[:, 1:2] / whole - average * average
+            v = (filt[rs_, :] - average) * lax.rsqrt(variance + EPSILON) * ln_gain[...] + ln_bias[
+                ...
+            ]
+            act[rs_, :] = (v / (1.0 + jnp.exp(-v))).astype(BF)
+
+    def mix():
+        loads[4].wait()
+
+        def outer(ks):
+            r = jnp.dot(act[...], proj[:, ks], preferred_element_type=F32).astype(BF)
+            for b in range(4):
+                part[b, 0:block, ks] = r[b * block : (b + 1) * block, :]
+
+        tiles(wide // 512, 512, outer)
+
+    wing = wide // 2
+    right, left, across = column(1), column(3), column(2)
+
+    def reduce_copy(n):
+        source = [
+            part.at[across, :, pl.ds(0, wing)],
+            part.at[across, :, pl.ds(wing, wing)],
+            part.at[right],
+            part.at[left],
+        ][n]
+        target = [first.at[0], first.at[1], second.at[0], second.at[1]][n]
+        return pltpu.make_async_remote_copy(
+            src_ref=source,
+            dst_ref=target,
+            send_sem=qs.at[n],
+            recv_sem=qr.at[n],
+            device_id={"tp": right if n % 2 == 0 else left},
+            device_id_type=MESH,
+        )
+
+    def reduce_start():
+        reduce_copy(0).start()
+        reduce_copy(1).start()
+
+    def reduce_pass():
+        for n, owner in ((0, right), (1, left)):
+            reduce_copy(n).wait_recv()
+            for k in range(wing // 512):
+                ks = slice(n * wing + 512 * k, n * wing + 512 * k + 512)
+                part[owner, :, ks] = (
+                    part[owner, :, ks].astype(F32)
+                    + first[n, :, 512 * k : 512 * k + 512].astype(F32)
+                ).astype(BF)
+            reduce_copy(n + 2).start()
+
+    def reduce_end():
+        reduce_copy(2).wait_recv()
+        reduce_copy(3).wait_recv()
+
+        def body(ks):
+            second[0, :, ks] = (
+                part[t, :, ks].astype(F32)
+                + second[0, :, ks].astype(F32)
+                + second[1, :, ks].astype(F32)
+            ).astype(BF)
+
+        tiles(wide // 512, 512, body)
+        for piece in result:
+            piece.start()
+
+    result = [
+        pltpu.make_async_copy(second.at[0, pl.ds(0, block)], mixer_out, sem_local.at[10]),
+        pltpu.make_async_copy(second.at[0, pl.ds(block, block)], shared_out, sem_local.at[11]),
+    ]
 
     def receive(g):
         for i in range(8 * g, 8 * g + 8):
@@ -154,19 +381,16 @@
             forward(i).wait_recv()
         span = pl.ds(g * group, group)
         acc[...] = jnp.zeros_like(acc)
-        step = 1024
-
-        def body(k, carry):
-            ks = pl.ds(pl.multiple_of(k * step, step), step)
+
+        def body(ks):
             x = inbox[span, ks]
-            acc[:, 0:units] += jnp.dot(x, gate[ks, :], preferred_element_type=F32)
-            acc[:, units : 2 * units] += jnp.dot(x, up[ks, :], preferred_element_type=F32)
-            return carry
-
-        lax.fori_loop(0, depth // step, body, 0)
-        a = acc[:, 0:units]
+            acc[0:group, 0:units] += jnp.dot(x, gate[ks, :], preferred_element_type=F32)
+            acc[0:group, units : 2 * units] += jnp.dot(x, up[ks, :], preferred_element_type=F32)
+
+        tiles(depth // 1024, 1024, body)
+        a = acc[0:group, 0:units]
         hid[span, features(t, units)] = (
-            a * (1.0 / (1.0 + jnp.exp(-a))) * acc[:, units : 2 * units]
+            a * (1.0 / (1.0 + jnp.exp(-a))) * acc[0:group, units : 2 * units]
         ).astype(BF)
         for j in range(1, 4):
             hidden_copy(g, j).start()
@@ -191,8 +415,15 @@
             else:
                 give_back(i).start()
 
+    shared_expert()
+    convolve()
     receive(0)
+    activate()
+    mix()
+    reduce_start()
     receive(1)
+    loads[5].wait()
+    loads[6].wait()
     hidden(0)
     receive(2)
     hidden(1)
@@ -206,6 +437,16 @@
     hidden(3)
     project(2)
     project(3)
+    reduce_pass()
+    reduce_end()
+
+    rim_copy.wait_send()
+    for j in range(1, 4):
+        stats_copy(j).wait_send()
+    for n in range(4):
+        reduce_copy(n).wait_send()
+    for piece in result:
+        piece.wait()
 
     for i in range(1, 32):
         dispatch(i).wait_send()
@@ -219,26 +460,56 @@
         give_back(i).wait()
 
 
-def routed_rows(outbox, gate, up, down):
+def routed_rows(outbox, normed, mixer, weights):
     count, rows, half = outbox.shape
-    depth, units = gate.shape
-    width = down.shape[1] // 4
+    depth, units = weights[0].shape
+    width = weights[2].shape[1] // 4
     total = count * rows
+    length, channels = mixer[0].shape
+    wide = weights[2].shape[1]
+    block = length // 4
     dma = pltpu.SemaphoreType.DMA
     vmem = pl.BlockSpec(memory_space=pltpu.VMEM)
     hbm = pl.BlockSpec(memory_space=pl.ANY)
     return pl.pallas_call(
         expert_kernel,
-        out_shape=jax.ShapeDtypeStruct((count, rows, width), BF),
-        in_specs=[hbm, vmem, vmem, hbm],
-        out_specs=hbm,
+        out_shape=(
+            jax.ShapeDtypeStruct((count, rows, width), BF),
+            jax.ShapeDtypeStruct((block, wide), BF),
+            jax.ShapeDtypeStruct((block, wide), BF),
+        ),
+        in_specs=[hbm, hbm] + [vmem] * 6 + [hbm] * 7,
+        out_specs=(hbm, hbm, hbm),
         scratch_shapes=[
             pltpu.VMEM((total, depth), BF),
             pltpu.VMEM((total, 4 * units), BF),
             pltpu.VMEM((4 * units, width), BF),
             pltpu.VMEM((total, width), BF),
-            pltpu.VMEM((total // 4, 2 * units), F32),
-            dma((3,)),
+            pltpu.VMEM((length, 2 * units), F32),
+            pltpu.VMEM((depth, units), BF),
+            pltpu.VMEM((depth, units), BF),
+            pltpu.VMEM((length + 32, channels), F32),
+            pltpu.VMEM((length, channels), F32),
+            pltpu.VMEM((length, channels), BF),
+            pltpu.VMEM((32, channels), BF),
+            pltpu.VMEM((32, channels), BF),
+            pltpu.VMEM((4, 8, length), F32),
+            pltpu.VMEM((channels, wide), BF),
+            pltpu.VMEM((length, wide), BF),
+            pltpu.VMEM((depth, units), BF),
+            pltpu.VMEM((depth, units), BF),
+            pltpu.VMEM((units, wide), BF),
+            pltpu.VMEM((length, units), BF),
+            pltpu.VMEM((4, 2 * block, wide), BF),
+            pltpu.VMEM((2, 2 * block, wide // 2), BF),
+            pltpu.VMEM((2, 2 * block, wide), BF),
+            dma((12,)),
+            dma((1,)),
+            dma((1,)),
+            dma((4,)),
+            dma((4,)),
+            dma((4,)),
+            dma((4,)),
             dma((32,)),
             dma((32,)),
             dma((32,)),
@@ -251,30 +522,9 @@
             dma((32,)),
         ],
         compiler_params=pltpu.CompilerParams(
-            collective_id=0, has_side_effects=True, vmem_limit_bytes=56 * 1024 * 1024
+            collective_id=0, has_side_effects=True, vmem_limit_bytes=67_043_328
         ),
-        cost_estimate=pl.CostEstimate(
-            flops=150_000_000_000, bytes_accessed=32 * 1024 * 1024, transcendentals=0
-        ),
-    )(outbox, gate, up, down)
-
-
-def shifted(x, axis, by):
-    devices = lax.axis_size(axis)
-    pairs = [(i, i + by) for i in range(devices) if 0 <= i + by < devices]
-    return lax.ppermute(x, axis, pairs)
-
-
-def tap_filter(value_in, gate_in, conv_taps, conv_bias):
-    gated = (value_in.astype(F32) * jax.nn.sigmoid(gate_in.astype(F32))).astype(BF)
-    rim = conv_taps.shape[0] - 1
-    length = gated.shape[0]
-    before = shifted(gated[length - rim :], "ep", 1)
-    padded = jnp.concatenate([before, gated], axis=0).astype(F32)
-    filtered = jnp.zeros(gated.shape, F32) + conv_bias[None, :]
-    for tap in range(rim + 1):
-        filtered = filtered + conv_taps[tap][None, :] * padded[tap : tap + length]
-    return filtered
+    )(outbox, normed, *mixer, *weights)
 
 
 def per_device(
@@ -337,26 +587,27 @@
     outbox = jnp.dot(select, part, preferred_element_type=F32).astype(BF)
     outbox = outbox.reshape(ep_count, tp_count * CAP, half)
 
-    filtered = tap_filter(value_in, gate_in, conv_taps, conv_bias)
-    sums = jnp.stack([jnp.sum(filtered, axis=1), jnp.sum(filtered * filtered, axis=1)])
-    sums = jnp.sum(lax.all_gather(sums, "tp", axis=0), axis=0)
-    channel_count = filtered.shape[1] * tp_count
-    average = sums[0] / channel_count
-    variance = sums[1] / channel_count - average * average
-    normed_a = (filtered - average[:, None]) * lax.rsqrt(
-        variance[:, None] + EPSILON
-    ) * ln_gain + ln_bias
-    activated = jax.nn.silu(normed_a).astype(BF)
-    mixer_part = jnp.dot(activated, out_proj, preferred_element_type=F32).astype(BF)
-    shared_hidden = (
-        jax.nn.silu(jnp.dot(normed_b, shared_gate, preferred_element_type=F32))
-        * jnp.dot(normed_b, shared_up, preferred_element_type=F32)
-    ).astype(BF)
-    shared_part = jnp.dot(shared_hidden, shared_down, preferred_element_type=F32).astype(BF)
-    mixer_rows = lax.psum_scatter(mixer_part, "tp", scatter_dimension=0, tiled=True)
-    shared_rows = lax.psum_scatter(shared_part, "tp", scatter_dimension=0, tiled=True)
-
-    returned = routed_rows(outbox, expert_gate[0], expert_up[0], expert_down[0])
+    returned, mixer_rows, shared_rows = routed_rows(
+        outbox,
+        normed_b,
+        (
+            value_in,
+            gate_in,
+            conv_taps,
+            conv_bias[None, :],
+            ln_gain[None, :],
+            ln_bias[None, :],
+            out_proj,
+        ),
+        (
+            expert_gate[0],
+            expert_up[0],
+            expert_down[0],
+            shared_gate,
+            shared_up,
+            shared_down,
+        ),
+    )
     returned = returned.reshape(slot_count, -1)
     spread = jnp.where(ids[None, :] == slots[:, 0:1], weights[:, 0:1], 0.0) + jnp.where(
         ids[None, :] == slots[:, 1:2], weights[:, 1:2], 0.0

time: 301 us -> 294 us (0.977)
  the two profiles are of different devices: /device:TPU:1 before, /device:TPU:104 now
where the time goes in v2:
time: 294 us
  Pallas kernels  237 us (81%)
  matrix products  13.1 us (4%)
  blocking collectives  11.1 us (4%)
  waiting for transfers between devices  10.9 us (4%)
  other arithmetic  10.1 us (3%)
  starting transfers between devices  7.03 us (2%)
  local copies, waits for them, and re-layouts  3.73 us (1%)
    pallas_call x1, Pallas kernels, routed_rows(): pl.pallas_call(expert_kernel, out_shape=(jax.ShapeDtypeStruct((count, row...  237 us
    all_gather x1, blocking collectives, per_device(): lax.all_gather(jnp.concatenate([routes.astype(F32), route_weights], axis=...  11.1 us
    all_to_all x1, waiting for transfers between devices, per_device(): lax.all_to_all(combined.astype(BF).reshape(tp_count, rows_own, -1), 'tp',...  10.9 us
    all_to_all x1, starting transfers between devices, per_device(): lax.all_to_all(combined.astype(BF).reshape(tp_count, rows_own, -1), 'tp',...  7.03 us
  transfers between devices with their start and end apart: 1, of which 1 were waited for; matrix products, arithmetic and copies ran while one was open for 0% of the time, Pallas kernels for 0%

profile of v2, /device:TPU:104, one launch (start us, length us, event | category | flops | bytes accessed | tf_op | source)
XLA Modules:
  0.0 293.9 jit_solution(3734028433827153361)
XLA Ops:
  0.6 0.7 convert_element_type.57
  1.3 0.7 pad_maximum_fusion
  2.0 11.1 %all-gather = f32[512,4]{0,1:T(4,128)S(1)} all-gather(f32[128,4]{0,1:T(4,128)S(1)} %pad_maximum_fusion), channel_id=2, replica_groups=mesh['ep'=32,'tp'=4] {'tp'}, dimensions={0}, use_global_device_ids=true | all-gather | bytes 10240 | tf_op jit(solution)/shard_map/all_gather | solution.py:556
  13.2 0.2 copy.33
  13.5 0.1 broadcast_bitcast_fusion
  13.6 3.1 %fusion = f32[512]{0:T(512)S(1)} fusion(bf16[512,4096]{1,0:T(8,128)(2,1)} %param.24), kind=kLoop, calls=%fused_computation.2 | loop fusion | flops 6290944 | bytes 4196352 | tf_op jit(solution)/shard_map/reduce_sum | solution.py:578
  16.7 0.6 fusion.26
  17.3 0.1 copy.31
  17.3 0.2 fusion.18
  17.6 1.0 copy.30
  18.6 0.2 convert_element_type.62
  18.8 0.1 bitcast_add_fusion
  19.0 0.3 slice_reduce_fusion.1
  19.3 3.8 %fusion.2.normed = bf16[512,4096]{1,0:T(8,128)(2,1)S(1)} fusion(bf16[512,4096]{1,0:T(8,128)(2,1)} %param.24, f32[4096]{0:T(1024)S(1)} %copy-done.3, f32[512]{0:T(512)S(1)} %add_rsqrt_fusion), kind=kLoop, calls=%fused_computation.4 | loop fusion | flops 8388608 | bytes 8407040 | tf_op jit(solution)/shard_map/convert_element_type | solution.py:580
  23.2 5.5 %convolution_convert_fusion = bf16[1536,2048]{1,0:T(8,128)(2,1)} fusion(bf16[512,4096]{1,0:T(8,128)(2,1)S(1)} %fusion.2.normed, s32[]{:T(128)S(6)} %select_n.18, s32[512]{0:T(512)S(1)} %get-tuple-element.9, s32[512]{0:T(512)S(1)} %get-tuple-element.8), kind=kOutput, calls=%fused_computation.5 | convolution fusion | flops 3226730496 | bytes 8392708 | tf_op jit(solution)/shard_map/dot_general | solution.py:587
  28.7 237.0 %shard_map.176 = (bf16[32,48,1024]{2,1,0:T(8,128)(2,1)}, bf16[128,4096]{1,0:T(8,128)(2,1)}, bf16[128,4096]{1,0:T(8,128)(2,1)}) custom-call(bf16[32,48,2048]{2,1,0:T(8,128)(2,1)} %bitcast.41, bf16[512,4096]{1,0:T(8,128)(2,1)} %copy-done, bf16[512,512]{1,0:T(8,128)(2,1)} %value_in.1, bf16[512,512]{1,0:T(8,128)(2,1)} %gate_in.1, f32[31,512]{1,0:T(8,128)} %taps.1, ...), custom_call_target="tpu_custom_call" | custom-call | tf_op jit(solution)/shard_map/pallas_call | solution.py:474
  265.8 4.1 %fusion.7 = f32[512,1024]{1,0:T(8,128)S(1)} fusion(bf16[1536,1024]{1,0:T(8,128)(2,1)} %bitcast.54, f32[512]{0:T(512)} %bitcast.52, s32[512]{0:T(512)} %copy-done.6, f32[512]{0:T(512)} %bitcast.50, s32[512]{0:T(512)} %copy-done.4), kind=kOutput, calls=%fused_computation.18 | convolution fusion | flops 1617690624 | bytes 5251072 | tf_op jit(solution)/shard_map/dot_general | solution.py:617
  270.0 3.2 %add_convert_fusion.1 = bf16[512,1024]{1,0:T(8,128)(2,1)} fusion(f32[512,1024]{1,0:T(8,128)S(1)} %fusion.7, bf16[1536,1024]{1,0:T(8,128)(2,1)S(1)} %bitcast.55, f32[512]{0:T(512)S(1)} %bitcast.53, s32[512]{0:T(512)S(1)} %copy-done.7, f32[512]{0:T(512)S(1)} %bitcast.51, s32[512]{0:T(512)S(1)} %copy-done.5), kind=kOutput, calls=%fused_computation.16 | convolution fusion | flops 1616379904 | bytes 6299648 | tf_op jit(solution)/shard_map/dot_general | solution.py:617
  273.2 7.0 %all-to-all-start = ((bf16[4,128,1024]{2,1,0:T(8,128)(2,1)}), bf16[4,128,1024]{2,1,0:T(8,128)(2,1)S(1)}, u32[]{:S(2)}, u32[]{:S(2)}) async-start(bf16[4,128,1024]{2,1,0:T(8,128)(2,1)} %bitcast.15), calls=%async_computation | async-start | bytes 2097152 | tf_op jit(solution)/shard_map/all_to_all | solution.py:620
  280.3 10.9 %all-to-all-done = bf16[4,128,1024]{2,1,0:T(8,128)(2,1)S(1)} async-done(((bf16[4,128,1024]{2,1,0:T(8,128)(2,1)}), bf16[4,128,1024]{2,1,0:T(8,128)(2,1)S(1)}, u32[]{:S(2)}, u32[]{:S(2)}) %all-to-all-start) | async-done | bytes 1048608 | tf_op jit(solution)/shard_map/all_to_all | solution.py:620
  291.2 0.2 convert_bitcast_fusion
  291.4 0.2 copy.34
  291.7 1.2 add_convert_fusion
  292.9 1.0 copy.39
  (31 shorter events, 0.3 us)
Async XLA Ops:
  13.6 5.8 %copy-start.3 = (f32[4096]{0:T(1024)S(1)}, f32[4096]{0:T(1024)}, u32[]{:S(2)}) copy-start(f32[4096]{0:T(1024)} %param.25) | copy-start | bytes 49156
  19.3 3.9 %copy-start.4 = (s32[512]{0:T(512)}, s32[512]{0:T(512)S(1)}, u32[]{:S(2)}) copy-start(s32[512]{0:T(512)S(1)} %get-tuple-element.8) | copy-start | bytes 6148
  19.3 3.9 %copy-start.6 = (s32[512]{0:T(512)}, s32[512]{0:T(512)S(1)}, u32[]{:S(2)}) copy-start(s32[512]{0:T(512)S(1)} %get-tuple-element.9) | copy-start | bytes 6148
  23.2 5.6 %copy-start = (bf16[512,4096]{1,0:T(8,128)(2,1)}, bf16[512,4096]{1,0:T(8,128)(2,1)S(1)}, u32[]{:S(2)}) copy-start(bf16[512,4096]{1,0:T(8,128)(2,1)S(1)} %fusion.2.normed) | copy-start | bytes 12582916
  265.8 4.2 %copy-start.5 = (s32[512]{0:T(512)S(1)}, s32[512]{0:T(512)}, u32[]{:S(2)}) copy-start(s32[512]{0:T(512)} %copy-done.4) | copy-start | bytes 6148
  265.8 4.2 %copy-start.7 = (s32[512]{0:T(512)S(1)}, s32[512]{0:T(512)}, u32[]{:S(2)}) copy-start(s32[512]{0:T(512)} %copy-done.6) | copy-start | bytes 6148
  265.8 4.2 %copy-start.8 = (f32[512,1]{0,1:T(1,128)S(1)}, f32[512,1]{0,1:T(1,128)}, u32[]{:S(2)}) copy-start(f32[512,1]{0,1:T(1,128)} %get-tuple-element.12) | copy-start | bytes 6148
  265.8 4.2 %copy-start.9 = (f32[512,1]{0,1:T(1,128)S(1)}, f32[512,1]{0,1:T(1,128)}, u32[]{:S(2)}) copy-start(f32[512,1]{0,1:T(1,128)} %get-tuple-element.13) | copy-start | bytes 6148
  265.8 4.2 %copy-start.10 = (bf16[32,48,1024]{2,1,0:T(8,128)(2,1)S(1)}, bf16[32,48,1024]{2,1,0:T(8,128)(2,1)}, u32[]{:S(2)}) copy-start(bf16[32,48,1024]{2,1,0:T(8,128)(2,1)} %get-tuple-element.7) | copy-start | bytes 9437188
  273.2 17.9 %all-to-all-start = ((bf16[4,128,1024]{2,1,0:T(8,128)(2,1)}), bf16[4,128,1024]{2,1,0:T(8,128)(2,1)S(1)}, u32[]{:S(2)}, u32[]{:S(2)}) async-start(bf16[4,128,1024]{2,1,0:T(8,128)(2,1)} %bitcast.15), calls=%async_computation | async-start | bytes 2097152 | tf_op jit(solution)/shard_map/all_to_all | solution.py:620
  280.3 11.4 %copy-start.2 = (bf16[128,4096]{1,0:T(8,128)(2,1)S(1)}, bf16[128,4096]{1,0:T(8,128)(2,1)}, u32[]{:S(2)}) copy-start(bf16[128,4096]{1,0:T(8,128)(2,1)} %get-tuple-element.6) | copy-start | bytes 3145732
  291.6 1.3 copy-start.1

commit v3 on v2

--- a/solution.py
+++ b/solution.py
@@ -10,6 +10,15 @@
 EPSILON = 1e-06
 MESH = pl.DeviceIdType.MESH
 CAP = 12
+EDGE = 1024
+PAIRS = [
+    (0, 0), (0, 1), (1, 0), (0, 3),
+    (3, 0), (1, 1), (3, 1), (0, 2),
+    (2, 0), (2, 1), (1, 3), (3, 3),
+    (2, 3), (1, 2), (3, 2), (2, 2),
+]
+TURNS = [n for n, (a, b) in enumerate(PAIRS) if a and b]
+STRAIGHT = [n for n, (a, b) in enumerate(PAIRS) if (a or b) and not (a and b)]
 BF = jnp.bfloat16
 F32 = jnp.float32
 
@@ -33,6 +42,8 @@
     ret,
     mixer_out,
     shared_out,
+    corner,
+    corner_back,
     inbox,
     hid,
     wdn,
@@ -72,29 +83,39 @@
     wr,
     rs,
     rr,
+    ks,
+    kr,
+    bs,
+    br,
 ):
     me = lax.axis_index("ep")
     t = lax.axis_index("tp")
     z, y, c = me // 8, (me // 2) % 4, me % 2
     p = t % 2
     rows = outbox.shape[1]
-    half = outbox.shape[2]
+    sent = outbox.shape[2]
+    rest = gate.shape[0] - sent
+    mine = pl.ds(pl.multiple_of((1 - p) * rest, 128), sent)
+    lacking = pl.ds(pl.multiple_of((1 - p) * sent, 128), rest)
     group = 8 * rows
     units = gate.shape[1]
     width = wdn.shape[1]
     depth = gate.shape[0]
 
-    def offset(i):
-        dy = (i // 2) % 4
-        return (i // 8 + dy) % 4, dy, i % 2
+    def away(dz, dy, dc):
+        return ((z + 4 + dz) % 4) * 8 + ((y + 4 + dy) % 4) * 2 + (c + dc) % 2
 
     def ahead(i):
-        dz, dy, dc = offset(i)
-        return ((z + dz) % 4) * 8 + ((y + dy) % 4) * 2 + (c + dc) % 2
+        dz, dy = PAIRS[i // 2]
+        return away(dz, dy, i % 2)
 
     def behind(i):
-        dz, dy, dc = offset(i)
-        return ((z + 4 - dz) % 4) * 8 + ((y + 4 - dy) % 4) * 2 + (c + dc) % 2
+        dz, dy = PAIRS[i // 2]
+        return away(-dz, -dy, i % 2)
+
+    def legs(n):
+        dz, dy = PAIRS[n]
+        return ((0, dy), (dz, 0)) if (dz + dy) % 2 == 0 else ((dz, 0), (0, dy))
 
     def column(j):
         return (t + j) % 4
@@ -137,21 +158,77 @@
         down.at[:, features(t, width)], wdn.at[features(t, units), :], sem_local.at[0]
     )
     own_rows = pltpu.make_async_copy(
-        outbox.at[me], inbox.at[pl.ds(0, rows), features(p, half)], sem_local.at[1]
+        outbox.at[me], inbox.at[pl.ds(0, rows), mine], sem_local.at[1]
     )
 
     def dispatch(i):
         return pltpu.make_async_remote_copy(
             src_ref=outbox.at[ahead(i)],
-            dst_ref=inbox.at[pl.ds(i * rows, rows), features(p, half)],
+            dst_ref=inbox.at[pl.ds(i * rows, rows), mine],
             send_sem=ds.at[i],
             recv_sem=dr.at[i],
             device_id={"ep": ahead(i)},
             device_id_type=MESH,
         )
 
+    def to_corner(n):
+        dz, dy = PAIRS[n]
+        start = ((z + dz) % 4) * 8 + ((y + dy) % 4) * 2
+        k = TURNS.index(n)
+        leg = legs(n)[0]
+        return pltpu.make_async_remote_copy(
+            src_ref=outbox.at[pl.ds(start, 2)],
+            dst_ref=corner.at[k],
+            send_sem=ks.at[k],
+            recv_sem=kr.at[k],
+            device_id={"ep": away(*leg, 0)},
+            device_id_type=MESH,
+        )
+
+    def from_corner(i):
+        k = TURNS.index(i // 2)
+        leg = legs(i // 2)[1]
+        return pltpu.make_async_remote_copy(
+            src_ref=corner.at[k, (c + i % 2) % 2],
+            dst_ref=inbox.at[pl.ds(i * rows, rows), mine],
+            send_sem=ds.at[i],
+            recv_sem=dr.at[i],
+            device_id={"ep": away(*leg, i % 2)},
+            device_id_type=MESH,
+        )
+
+    def arrival(i):
+        return from_corner(i) if i // 2 in TURNS else dispatch(i)
+
+    def back_to_corner(n):
+        k = TURNS.index(n)
+        leg = legs(n)[0]
+        return pltpu.make_async_remote_copy(
+            src_ref=outs.at[pl.ds(n * 2 * rows, 2 * rows), :],
+            dst_ref=corner_back.at[k],
+            send_sem=bs.at[k],
+            recv_sem=br.at[k],
+            device_id={"ep": away(-leg[0], -leg[1], 0)},
+            device_id_type=MESH,
+        )
+
+    def back_from_corner(i):
+        k = TURNS.index(i // 2)
+        one, two = legs(i // 2)
+        return pltpu.make_async_remote_copy(
+            src_ref=corner_back.at[k, pl.ds((i % 2) * rows, rows)],
+            dst_ref=ret.at[away(*one, 0)],
+            send_sem=rs.at[i],
+            recv_sem=rr.at[i],
+            device_id={"ep": away(-two[0], -two[1], i % 2)},
+            device_id_type=MESH,
+        )
+
+    def return_leg(i):
+        return back_from_corner(i) if i // 2 in TURNS else give_back(i)
+
     def forward(i):
-        place = inbox.at[pl.ds(i * rows, rows), features(p, half)]
+        place = inbox.at[pl.ds(i * rows, rows), lacking]
         return pltpu.make_async_remote_copy(
             src_ref=place,
             dst_ref=place,
@@ -162,13 +239,18 @@
         )
 
     def hidden_copy(g, j):
-        place = hid.at[pl.ds(g * group, group), features(t, units)]
+        to = j
+        source = t
+        if j == 2:
+            to = 1 if g % 2 == 0 else 3
+            source = column(4 - to)
+        place = hid.at[pl.ds(g * group, group), features(source, units)]
         return pltpu.make_async_remote_copy(
             src_ref=place,
             dst_ref=place,
             send_sem=hs.at[g, j],
             recv_sem=hr.at[g, j],
-            device_id={"tp": column(j)},
+            device_id={"tp": column(to)},
             device_id_type=MESH,
         )
 
@@ -185,8 +267,15 @@
     own_back = pltpu.make_async_copy(outs.at[pl.ds(0, rows), :], ret.at[me], sem_local.at[2])
 
     own_rows.start()
-    for i in range(1, 32):
-        dispatch(i).start()
+    dispatch(1).start()
+    straight = list(STRAIGHT)
+    for count, n in enumerate(TURNS):
+        to_corner(n).start()
+        if count % 3 == 0:
+            for _ in range(2):
+                m = straight.pop(0)
+                dispatch(2 * m).start()
+                dispatch(2 * m + 1).start()
     own_weight.start()
     for j in range(1, 4):
         weight_copy(j).start()
@@ -316,14 +405,16 @@
     wing = wide // 2
     right, left, across = column(1), column(3), column(2)
 
+    piece = block // 2
+
     def reduce_copy(n):
-        source = [
-            part.at[across, :, pl.ds(0, wing)],
-            part.at[across, :, pl.ds(wing, wing)],
-            part.at[right],
-            part.at[left],
-        ][n]
-        target = [first.at[0], first.at[1], second.at[0], second.at[1]][n]
+        if n < 2:
+            source = part.at[across, :, pl.ds(n * wing, wing)]
+            target = first.at[n]
+        else:
+            span = pl.ds((n // 2 - 1) * piece, piece)
+            source = part.at[right if n % 2 == 0 else left, span]
+            target = second.at[n % 2, span]
         return pltpu.make_async_remote_copy(
             src_ref=source,
             dst_ref=target,
@@ -337,20 +428,23 @@
         reduce_copy(0).start()
         reduce_copy(1).start()
 
-    def reduce_pass():
+    def reduce_pass(q):
+        if q == 0:
+            reduce_copy(0).wait_recv()
+            reduce_copy(1).wait_recv()
+        span = pl.ds(q * piece, piece)
         for n, owner in ((0, right), (1, left)):
+            for k in range(wing // 512):
+                cols = slice(n * wing + 512 * k, n * wing + 512 * k + 512)
+                part[owner, span, cols] = (
+                    part[owner, span, cols].astype(F32)
+                    + first[n, span, 512 * k : 512 * k + 512].astype(F32)
+                ).astype(BF)
+            reduce_copy(2 * q + 2 + n).start()
+
+    def reduce_end():
+        for n in range(2, 10):
             reduce_copy(n).wait_recv()
-            for k in range(wing // 512):
-                ks = slice(n * wing + 512 * k, n * wing + 512 * k + 512)
-                part[owner, :, ks] = (
-                    part[owner, :, ks].astype(F32)
-                    + first[n, :, 512 * k : 512 * k + 512].astype(F32)
-                ).astype(BF)
-            reduce_copy(n + 2).start()
-
-    def reduce_end():
-        reduce_copy(2).wait_recv()
-        reduce_copy(3).wait_recv()
 
         def body(ks):
             second[0, :, ks] = (
@@ -360,8 +454,8 @@
             ).astype(BF)
 
         tiles(wide // 512, 512, body)
-        for piece in result:
-            piece.start()
+        for copy in result:
+            copy.start()
 
     result = [
         pltpu.make_async_copy(second.at[0, pl.ds(0, block)], mixer_out, sem_local.at[10]),
@@ -373,7 +467,7 @@
             if i == 0:
                 own_rows.wait()
             else:
-                dispatch(i).wait_recv()
+                arrival(i).wait_recv()
             forward(i).start()
 
     def hidden(g):
@@ -392,12 +486,16 @@
         hid[span, features(t, units)] = (
             a * (1.0 / (1.0 + jnp.exp(-a))) * acc[0:group, units : 2 * units]
         ).astype(BF)
-        for j in range(1, 4):
-            hidden_copy(g, j).start()
+        hidden_copy(g, 1).start()
+        hidden_copy(g, 3).start()
+
+    def pass_hidden(g):
+        hidden_copy(g, 1).wait_recv()
+        hidden_copy(g, 3).wait_recv()
+        hidden_copy(g, 2).start()
 
     def project(g):
-        for j in range(1, 4):
-            hidden_copy(g, j).wait_recv()
+        hidden_copy(g, 2).wait_recv()
         span = pl.ds(g * group, group)
         step = 256
 
@@ -409,47 +507,80 @@
             return carry
 
         lax.fori_loop(0, width // step, body, 0)
-        for i in range(8 * g, 8 * g + 8):
-            if i == 0:
-                own_back.start()
+        for n in range(4 * g, 4 * g + 4):
+            if n in TURNS:
+                back_to_corner(n).start()
             else:
-                give_back(i).start()
+                if n == 0:
+                    own_back.start()
+                else:
+                    give_back(2 * n).start()
+                give_back(2 * n + 1).start()
+
+    def turn(ks_):
+        for k in ks_:
+            to_corner(TURNS[k]).wait_recv()
+            from_corner(2 * TURNS[k]).start()
+            from_corner(2 * TURNS[k] + 1).start()
+
+    def turn_back(g):
+        for n in range(4 * g, 4 * g + 4):
+            if n in TURNS:
+                back_to_corner(n).wait_recv()
+                back_from_corner(2 * n).start()
+                back_from_corner(2 * n + 1).start()
 
     shared_expert()
+    turn(range(0, 2))
     convolve()
+    turn(range(2, 4))
     receive(0)
     activate()
+    turn(range(4, 6))
     mix()
+    turn(range(6, 9))
     reduce_start()
     receive(1)
     loads[5].wait()
     loads[6].wait()
     hidden(0)
     receive(2)
+    pass_hidden(0)
     hidden(1)
     own_weight.wait()
     for j in range(1, 4):
         weight_copy(j).wait()
+    reduce_pass(0)
     project(0)
     receive(3)
+    pass_hidden(1)
     hidden(2)
+    reduce_pass(1)
     project(1)
+    pass_hidden(2)
     hidden(3)
+    turn_back(1)
     project(2)
+    pass_hidden(3)
+    reduce_pass(2)
     project(3)
-    reduce_pass()
+    reduce_pass(3)
+    turn_back(2)
+    turn_back(3)
     reduce_end()
 
     rim_copy.wait_send()
     for j in range(1, 4):
         stats_copy(j).wait_send()
-    for n in range(4):
+    for n in range(10):
         reduce_copy(n).wait_send()
-    for piece in result:
-        piece.wait()
-
+    for copy in result:
+        copy.wait()
     for i in range(1, 32):
-        dispatch(i).wait_send()
+        arrival(i).wait_send()
+    for n in TURNS:
+        to_corner(n).wait_send()
+        back_to_corner(n).wait_send()
     for i in range(32):
         forward(i).wait_send()
     for g in range(4):
@@ -457,11 +588,11 @@
             hidden_copy(g, j).wait_send()
     own_back.wait()
     for i in range(1, 32):
-        give_back(i).wait()
+        return_leg(i).wait()
 
 
 def routed_rows(outbox, normed, mixer, weights):
-    count, rows, half = outbox.shape
+    count, rows, sent = outbox.shape
     depth, units = weights[0].shape
     width = weights[2].shape[1] // 4
     total = count * rows
@@ -477,9 +608,11 @@
             jax.ShapeDtypeStruct((count, rows, width), BF),
             jax.ShapeDtypeStruct((block, wide), BF),
             jax.ShapeDtypeStruct((block, wide), BF),
+            jax.ShapeDtypeStruct((len(TURNS), 2, rows, sent), BF),
+            jax.ShapeDtypeStruct((len(TURNS), 2 * rows, width), BF),
         ),
         in_specs=[hbm, hbm] + [vmem] * 6 + [hbm] * 7,
-        out_specs=(hbm, hbm, hbm),
+        out_specs=(hbm,) * 5,
         scratch_shapes=[
             pltpu.VMEM((total, depth), BF),
             pltpu.VMEM((total, 4 * units), BF),
@@ -508,8 +641,8 @@
             dma((1,)),
             dma((4,)),
             dma((4,)),
-            dma((4,)),
-            dma((4,)),
+            dma((10,)),
+            dma((10,)),
             dma((32,)),
             dma((32,)),
             dma((32,)),
@@ -520,6 +653,10 @@
             dma((4,)),
             dma((32,)),
             dma((32,)),
+            dma((9,)),
+            dma((9,)),
+            dma((9,)),
+            dma((9,)),
         ],
         compiler_params=pltpu.CompilerParams(
             collective_id=0, has_side_effects=True, vmem_limit_bytes=67_043_328
@@ -578,16 +715,16 @@
         * lax.rsqrt(jnp.mean(features * features, axis=1, keepdims=True) + EPSILON)
         * norm_gain
     ).astype(BF)
-    half = model_width // 2
-    part = lax.dynamic_slice_in_dim(normed_b, (t % 2) * half, half, 1)
+    sent = model_width - EDGE
+    part = lax.dynamic_slice_in_dim(normed_b, (1 - t % 2) * EDGE, sent, 1)
     ids = jnp.arange(slot_count, dtype=jnp.int32)
     select = (
         (ids[:, None] == slots[None, :, 0]) | (ids[:, None] == slots[None, :, 1])
     ).astype(BF)
     outbox = jnp.dot(select, part, preferred_element_type=F32).astype(BF)
-    outbox = outbox.reshape(ep_count, tp_count * CAP, half)
-
-    returned, mixer_rows, shared_rows = routed_rows(
+    outbox = outbox.reshape(ep_count, tp_count * CAP, sent)
+
+    returned, mixer_rows, shared_rows, _, _ = routed_rows(
         outbox,
         normed_b,
         (

time: 294 us -> 270 us (0.918)
  the two profiles are of different devices: /device:TPU:104 before, /device:TPU:1 now
where the time goes in v3:
time: 270 us
  Pallas kernels  211 us (78%)
  waiting for transfers between devices  15.5 us (6%)
  matrix products  15.4 us (6%)
  other arithmetic  10 us (4%)
  blocking collectives  9.3 us (3%)
  local copies, waits for them, and re-layouts  3.73 us (1%)
  starting transfers between devices  3.52 us (1%)
    pallas_call x1, Pallas kernels, routed_rows(): pl.pallas_call(expert_kernel, out_shape=(jax.ShapeDtypeStruct((count, row...  211 us
    all_to_all x1, waiting for transfers between devices, per_device(): lax.all_to_all(combined.astype(BF).reshape(tp_count, rows_own, -1), 'tp',...  15.5 us
    all_gather x1, blocking collectives, per_device(): lax.all_gather(jnp.concatenate([routes.astype(F32), route_weights], axis=...  9.3 us
    dot_general x1, matrix products, per_device(): outbox = jnp.dot(select, part, preferred_element_type=F32).astype(BF)  7.84 us
  transfers between devices with their start and end apart: 1, of which 1 were waited for; matrix products, arithmetic and copies ran while one was open for 0% of the time, Pallas kernels for 0%

profile of v3, /device:TPU:1, one launch (start us, length us, event | category | flops | bytes accessed | tf_op | source)
XLA Modules:
  0.0 269.9 jit_solution(129582843297976332)
XLA Ops:
  0.6 0.7 convert_element_type.57
  1.3 0.7 pad_maximum_fusion
  2.0 9.3 %all-gather = f32[512,4]{0,1:T(4,128)S(1)} all-gather(f32[128,4]{0,1:T(4,128)S(1)} %pad_maximum_fusion), channel_id=2, replica_groups=mesh['ep'=32,'tp'=4] {'tp'}, dimensions={0}, use_global_device_ids=true | all-gather | bytes 10240 | tf_op jit(solution)/shard_map/all_gather | solution.py:693
  11.3 0.2 copy.33
  11.6 0.1 broadcast_bitcast_fusion
  11.7 3.1 %fusion = f32[512]{0:T(512)S(1)} fusion(bf16[512,4096]{1,0:T(8,128)(2,1)} %param.24), kind=kLoop, calls=%fused_computation.3 | loop fusion | flops 6290944 | bytes 4196352 | tf_op jit(solution)/shard_map/reduce_sum | solution.py:715
  14.8 0.6 fusion.26
  15.4 0.1 copy.31
  15.5 0.2 fusion.18
  15.7 1.0 copy.30
  16.8 0.2 convert_element_type.62
  17.0 0.1 bitcast_add_fusion
  17.2 0.3 slice_reduce_fusion.1
  17.5 3.8 %fusion.2.normed = bf16[512,4096]{1,0:T(8,128)(2,1)S(1)} fusion(bf16[512,4096]{1,0:T(8,128)(2,1)} %param.24, f32[4096]{0:T(1024)S(1)} %copy-done.3, f32[512]{0:T(512)S(1)} %add_rsqrt_fusion), kind=kLoop, calls=%fused_computation.5 | loop fusion | flops 8388608 | bytes 8407040 | tf_op jit(solution)/shard_map/convert_element_type | solution.py:717
  21.4 7.8 %convolution_convert_fusion = bf16[1536,3072]{1,0:T(8,128)(2,1)} fusion(bf16[512,4096]{1,0:T(8,128)(2,1)S(1)} %fusion.2.normed, s32[]{:T(128)S(6)} %select_n.18, s32[512]{0:T(512)S(1)} %get-tuple-element.9, s32[512]{0:T(512)S(1)} %get-tuple-element.8), kind=kOutput, calls=%fused_computation | convolution fusion | flops 4838916096 | bytes 12587012 | tf_op jit(solution)/shard_map/dot_general | solution.py:724
  29.2 211.4 %shard_map.176 = (bf16[32,48,1024]{2,1,0:T(8,128)(2,1)}, bf16[128,4096]{1,0:T(8,128)(2,1)}, bf16[128,4096]{1,0:T(8,128)(2,1)}, bf16[9,2,48,3072]{3,2,1,0:T(8,128)(2,1)}, bf16[9,96,1024]{2,1,0:T(8,128)(2,1)}) custom-call(bf16[32,48,3072]{2,1,0:T(8,128)(2,1)} %bitcast.40, bf16[512,4096]{1,0:T(8,128)(2,1)} %copy-done, bf16[512,512]{1,0:T(8,128)(2,1)} %value_in.1, ...), custom_call_target="tpu_custom_call" | custom-call | tf_op jit(solution)/shard_map/pallas_call | solution.py:605
  240.7 4.1 %fusion.7 = f32[512,1024]{1,0:T(8,128)S(1)} fusion(bf16[1536,1024]{1,0:T(8,128)(2,1)} %bitcast.54, f32[512]{0:T(512)} %bitcast.52, s32[512]{0:T(512)} %copy-done.6, f32[512]{0:T(512)} %bitcast.50, s32[512]{0:T(512)} %copy-done.4), kind=kOutput, calls=%fused_computation.18 | convolution fusion | flops 1617690624 | bytes 5251072 | tf_op jit(solution)/shard_map/dot_general | solution.py:754
  244.9 3.2 %add_convert_fusion.1 = bf16[512,1024]{1,0:T(8,128)(2,1)} fusion(f32[512,1024]{1,0:T(8,128)S(1)} %fusion.7, bf16[1536,1024]{1,0:T(8,128)(2,1)S(1)} %bitcast.55, f32[512]{0:T(512)S(1)} %bitcast.53, s32[512]{0:T(512)S(1)} %copy-done.7, f32[512]{0:T(512)S(1)} %bitcast.51, s32[512]{0:T(512)S(1)} %copy-done.5), kind=kOutput, calls=%fused_computation.17 | convolution fusion | flops 1616379904 | bytes 6299648 | tf_op jit(solution)/shard_map/dot_general | solution.py:754
  248.1 3.5 %all-to-all-start = ((bf16[4,128,1024]{2,1,0:T(8,128)(2,1)}), bf16[4,128,1024]{2,1,0:T(8,128)(2,1)S(1)}, u32[]{:S(2)}, u32[]{:S(2)}) async-start(bf16[4,128,1024]{2,1,0:T(8,128)(2,1)} %bitcast.15), calls=%async_computation | async-start | bytes 2097152 | tf_op jit(solution)/shard_map/all_to_all | solution.py:757
  251.6 15.5 %all-to-all-done = bf16[4,128,1024]{2,1,0:T(8,128)(2,1)S(1)} async-done(((bf16[4,128,1024]{2,1,0:T(8,128)(2,1)}), bf16[4,128,1024]{2,1,0:T(8,128)(2,1)S(1)}, u32[]{:S(2)}, u32[]{:S(2)}) %all-to-all-start) | async-done | bytes 1048608 | tf_op jit(solution)/shard_map/all_to_all | solution.py:757
  267.1 0.2 convert_bitcast_fusion
  267.4 0.2 copy.34
  267.6 1.2 add_convert_fusion
  268.9 1.0 copy.39
  (31 shorter events, 0.2 us)
Async XLA Ops:
  11.7 5.8 %copy-start.3 = (f32[4096]{0:T(1024)S(1)}, f32[4096]{0:T(1024)}, u32[]{:S(2)}) copy-start(f32[4096]{0:T(1024)} %param.25) | copy-start | bytes 49156
  17.5 3.9 %copy-start.4 = (s32[512]{0:T(512)}, s32[512]{0:T(512)S(1)}, u32[]{:S(2)}) copy-start(s32[512]{0:T(512)S(1)} %get-tuple-element.8) | copy-start | bytes 6148
  17.5 3.9 %copy-start.6 = (s32[512]{0:T(512)}, s32[512]{0:T(512)S(1)}, u32[]{:S(2)}) copy-start(s32[512]{0:T(512)S(1)} %get-tuple-element.9) | copy-start | bytes 6148
  21.3 7.9 %copy-start = (bf16[512,4096]{1,0:T(8,128)(2,1)}, bf16[512,4096]{1,0:T(8,128)(2,1)S(1)}, u32[]{:S(2)}) copy-start(bf16[512,4096]{1,0:T(8,128)(2,1)S(1)} %fusion.2.normed) | copy-start | bytes 12582916
  240.6 4.2 %copy-start.5 = (s32[512]{0:T(512)S(1)}, s32[512]{0:T(512)}, u32[]{:S(2)}) copy-start(s32[512]{0:T(512)} %copy-done.4) | copy-start | bytes 6148
  240.6 4.2 %copy-start.7 = (s32[512]{0:T(512)S(1)}, s32[512]{0:T(512)}, u32[]{:S(2)}) copy-start(s32[512]{0:T(512)} %copy-done.6) | copy-start | bytes 6148
  240.6 4.2 %copy-start.8 = (f32[512,1]{0,1:T(1,128)S(1)}, f32[512,1]{0,1:T(1,128)}, u32[]{:S(2)}) copy-start(f32[512,1]{0,1:T(1,128)} %get-tuple-element.12) | copy-start | bytes 6148
  240.6 4.2 %copy-start.9 = (f32[512,1]{0,1:T(1,128)S(1)}, f32[512,1]{0,1:T(1,128)}, u32[]{:S(2)}) copy-start(f32[512,1]{0,1:T(1,128)} %get-tuple-element.13) | copy-start | bytes 6148
  240.7 4.2 %copy-start.10 = (bf16[32,48,1024]{2,1,0:T(8,128)(2,1)S(1)}, bf16[32,48,1024]{2,1,0:T(8,128)(2,1)}, u32[]{:S(2)}) copy-start(bf16[32,48,1024]{2,1,0:T(8,128)(2,1)} %get-tuple-element.7) | copy-start | bytes 9437188
  248.1 19.0 %all-to-all-start = ((bf16[4,128,1024]{2,1,0:T(8,128)(2,1)}), bf16[4,128,1024]{2,1,0:T(8,128)(2,1)S(1)}, u32[]{:S(2)}, u32[]{:S(2)}) async-start(bf16[4,128,1024]{2,1,0:T(8,128)(2,1)} %bitcast.15), calls=%async_computation | async-start | bytes 2097152 | tf_op jit(solution)/shard_map/all_to_all | solution.py:757
  251.6 16.0 %copy-start.2 = (bf16[128,4096]{1,0:T(8,128)(2,1)S(1)}, bf16[128,4096]{1,0:T(8,128)(2,1)}, u32[]{:S(2)}) copy-start(bf16[128,4096]{1,0:T(8,128)(2,1)} %get-tuple-element.6) | copy-start | bytes 3145732
  267.6 1.3 copy-start.1

commit v4 on v3

--- a/solution.py
+++ b/solution.py
@@ -39,9 +39,9 @@
     sgate_hbm,
     sup_hbm,
     sdown_hbm,
-    ret,
+    spread,
     mixer_out,
-    shared_out,
+    experts_out,
     corner,
     corner_back,
     inbox,
@@ -66,7 +66,10 @@
     part,
     first,
     second,
+    ret,
     sem_local,
+    xs,
+    xr,
     cs,
     cr,
     ss,
@@ -454,13 +457,57 @@
             ).astype(BF)
 
         tiles(wide // 512, 512, body)
-        for copy in result:
-            copy.start()
+        result[0].start()
 
     result = [
         pltpu.make_async_copy(second.at[0, pl.ds(0, block)], mixer_out, sem_local.at[10]),
-        pltpu.make_async_copy(second.at[0, pl.ds(block, block)], shared_out, sem_local.at[11]),
+        pltpu.make_async_copy(sdown.at[pl.ds(0, block)], experts_out, sem_local.at[11]),
     ]
+
+    load_spread = pltpu.make_async_copy(
+        spread, proj.at[:, pl.ds(0, spread.shape[1])], sem_local.at[12]
+    )
+
+    def quarter_copy(j):
+        return pltpu.make_async_remote_copy(
+            src_ref=nb.at[pl.ds(pl.multiple_of(column(j) * block, block), block), pl.ds(0, width)],
+            dst_ref=sdown.at[pl.ds(0, block), features(t, width)],
+            send_sem=xs.at[j],
+            recv_sem=xr.at[j],
+            device_id={"tp": column(j)},
+            device_id_type=MESH,
+        )
+
+    def combine(j):
+        span = pl.ds(pl.multiple_of(column(j) * block, block), block)
+        slots = hid.shape[0]
+        for k in range(2):
+            cols = slice(k * width // 2, (k + 1) * width // 2)
+            values = ret[:, :, cols].reshape(slots, width // 2)
+            total = jnp.dot(
+                proj[span, 0:slots], values, preferred_element_type=F32
+            ) + jnp.dot(proj[span, slots : 2 * slots], values, preferred_element_type=F32)
+            nb[span, cols] = total.astype(BF)
+
+    def finish():
+        for j in (2, 1, 3):
+            combine(j)
+            quarter_copy(j).start()
+        combine(0)
+        own = nb[pl.ds(pl.multiple_of(t * block, block), block), 0:width]
+        sdown[0:block, features(t, width)] = own
+
+    def last_sum():
+        for j in range(1, 4):
+            quarter_copy(j).wait_recv()
+
+        def body(cols):
+            sdown[0:block, cols] = (
+                second[0, block : 2 * block, cols].astype(F32) + sdown[0:block, cols].astype(F32)
+            ).astype(BF)
+
+        tiles(wide // 512, 512, body)
+        result[1].start()
 
     def receive(g):
         for i in range(8 * g, 8 * g + 8):
@@ -538,6 +585,7 @@
     activate()
     turn(range(4, 6))
     mix()
+    load_spread.start()
     turn(range(6, 9))
     reduce_start()
     receive(1)
@@ -567,15 +615,20 @@
     reduce_pass(3)
     turn_back(2)
     turn_back(3)
+    own_back.wait()
+    for i in range(1, 32):
+        return_leg(i).wait_recv()
+    load_spread.wait()
+    finish()
     reduce_end()
+    last_sum()
 
     rim_copy.wait_send()
     for j in range(1, 4):
         stats_copy(j).wait_send()
     for n in range(10):
         reduce_copy(n).wait_send()
-    for copy in result:
-        copy.wait()
+    result[0].wait()
     for i in range(1, 32):
         arrival(i).wait_send()
     for n in TURNS:
@@ -586,12 +639,65 @@
     for g in range(4):
         for j in range(1, 4):
             hidden_copy(g, j).wait_send()
-    own_back.wait()
     for i in range(1, 32):
-        return_leg(i).wait()
-
-
-def routed_rows(outbox, normed, mixer, weights):
+        return_leg(i).wait_send()
+    for j in range(1, 4):
+        quarter_copy(j).wait_send()
+    result[1].wait()
+
+
+def norm_kernel(table, tokens, gain, tables, normed, sends, receives):
+    t = lax.axis_index("tp")
+    barrier = pltpu.get_barrier_semaphore()
+    for j in range(1, 4):
+        pl.semaphore_signal(barrier, inc=1, device_id={"tp": (t + j) % 4}, device_id_type=MESH)
+    pl.semaphore_wait(barrier, 3)
+
+    def table_copy(j):
+        return pltpu.make_async_remote_copy(
+            src_ref=table,
+            dst_ref=tables.at[t],
+            send_sem=sends.at[j],
+            recv_sem=receives.at[j],
+            device_id={"tp": (t + j) % 4},
+            device_id_type=MESH,
+        )
+
+    for j in range(1, 4):
+        table_copy(j).start()
+    tables[t] = table[...]
+    size = 32
+
+    def body(k, carry):
+        span = pl.ds(pl.multiple_of(k * size, size), size)
+        x = tokens[span, :].astype(F32)
+        scale = lax.rsqrt(jnp.mean(x * x, axis=1, keepdims=True) + EPSILON)
+        normed[span, :] = (x * scale * gain[...]).astype(BF)
+        return carry
+
+    lax.fori_loop(0, tokens.shape[0] // size, body, 0)
+    for j in range(1, 4):
+        table_copy(j).wait()
+
+
+def normed_rows(table, tokens, gain):
+    vmem = pl.BlockSpec(memory_space=pltpu.VMEM)
+    return pl.pallas_call(
+        norm_kernel,
+        out_shape=(
+            jax.ShapeDtypeStruct((4, *table.shape), F32),
+            jax.ShapeDtypeStruct(tokens.shape, BF),
+        ),
+        in_specs=[vmem] * 3,
+        out_specs=(vmem, vmem),
+        scratch_shapes=[pltpu.SemaphoreType.DMA((4,)), pltpu.SemaphoreType.DMA((4,))],
+        compiler_params=pltpu.CompilerParams(
+            collective_id=1, has_side_effects=True, vmem_limit_bytes=24 * 1024 * 1024
+        ),
+    )(table, tokens, gain[None, :])
+
+
+def routed_rows(outbox, normed, mixer, weights, spread):
     count, rows, sent = outbox.shape
     depth, units = weights[0].shape
     width = weights[2].shape[1] // 4
@@ -605,14 +711,13 @@
     return pl.pallas_call(
         expert_kernel,
         out_shape=(
-            jax.ShapeDtypeStruct((count, rows, width), BF),
             jax.ShapeDtypeStruct((block, wide), BF),
             jax.ShapeDtypeStruct((block, wide), BF),
             jax.ShapeDtypeStruct((len(TURNS), 2, rows, sent), BF),
             jax.ShapeDtypeStruct((len(TURNS), 2 * rows, width), BF),
         ),
-        in_specs=[hbm, hbm] + [vmem] * 6 + [hbm] * 7,
-        out_specs=(hbm,) * 5,
+        in_specs=[hbm, hbm] + [vmem] * 6 + [hbm] * 8,
+        out_specs=(hbm,) * 4,
         scratch_shapes=[
             pltpu.VMEM((total, depth), BF),
             pltpu.VMEM((total, 4 * units), BF),
@@ -636,7 +741,10 @@
             pltpu.VMEM((4, 2 * block, wide), BF),
             pltpu.VMEM((2, 2 * block, wide // 2), BF),
             pltpu.VMEM((2, 2 * block, wide), BF),
-            dma((12,)),
+            pltpu.VMEM((count, rows, width), BF),
+            dma((13,)),
+            dma((4,)),
+            dma((4,)),
             dma((1,)),
             dma((1,)),
             dma((4,)),
@@ -661,7 +769,7 @@
         compiler_params=pltpu.CompilerParams(
             collective_id=0, has_side_effects=True, vmem_limit_bytes=67_043_328
         ),
-    )(outbox, normed, *mixer, *weights)
+    )(outbox, normed, *mixer, *weights, spread)
 
 
 def per_device(
@@ -690,31 +798,31 @@
     rows_all = rows_own * tp_count
     model_width = tokens_b.shape[1]
 
-    tables = lax.all_gather(
-        jnp.concatenate([routes.astype(F32), route_weights], axis=1), "tp", axis=0
+    own = jnp.concatenate(
+        [
+            routes.astype(F32).T,
+            route_weights.T,
+            jnp.zeros((8 - 2 * top_count, rows_own), F32),
+        ],
+        axis=0,
     )
-    chosen = tables[:, :, :top_count].astype(jnp.int32).reshape(tp_count, -1)
-    weights = tables[:, :, top_count:].reshape(rows_all, top_count)
-    onehot = (chosen[:, :, None] == jnp.arange(ep_count, dtype=jnp.int32)).astype(BF)
-    pairs = chosen.shape[1]
-    lower = (
-        jnp.arange(pairs, dtype=jnp.int32)[:, None] > jnp.arange(pairs, dtype=jnp.int32)[None, :]
-    ).astype(BF)
-    earlier = jnp.einsum("ij,bje->bie", lower, onehot, preferred_element_type=F32)
-    places = jnp.sum(earlier * onehot.astype(F32), axis=2).astype(jnp.int32)
+    tables, normed_b = normed_rows(own, tokens_b, norm_gain)
+    chosen = jnp.swapaxes(tables[:, 0:top_count, :], 1, 2).astype(jnp.int32)
+    weights = jnp.swapaxes(tables[:, top_count : 2 * top_count, :], 1, 2)
+    weights = weights.reshape(rows_all, top_count)
+    onehot = chosen[:, :, :, None] == jnp.arange(ep_count, dtype=jnp.int32)
+    named = jnp.sum(onehot.astype(F32), axis=2).astype(BF)
+    ranks = jnp.arange(rows_own, dtype=jnp.int32)
+    lower = (ranks[:, None] > ranks[None, :]).astype(BF)
+    earlier = jnp.einsum("ij,bje->bie", lower, named, preferred_element_type=F32)
+    places = jnp.sum(jnp.where(onehot, earlier[:, :, None, :], 0.0), axis=3).astype(jnp.int32)
     slots = (
         chosen * (tp_count * CAP)
-        + jnp.arange(tp_count, dtype=jnp.int32)[:, None] * CAP
+        + jnp.arange(tp_count, dtype=jnp.int32)[:, None, None] * CAP
         + places
     ).reshape(rows_all, top_count)
     slot_count = ep_count * tp_count * CAP
 
-    features = tokens_b.astype(F32)
-    normed_b = (
-        features
-        * lax.rsqrt(jnp.mean(features * features, axis=1, keepdims=True) + EPSILON)
-        * norm_gain
-    ).astype(BF)
     sent = model_width - EDGE
     part = lax.dynamic_slice_in_dim(normed_b, (1 - t % 2) * EDGE, sent, 1)
     ids = jnp.arange(slot_count, dtype=jnp.int32)
@@ -724,7 +832,12 @@
     outbox = jnp.dot(select, part, preferred_element_type=F32).astype(BF)
     outbox = outbox.reshape(ep_count, tp_count * CAP, sent)
 
-    returned, mixer_rows, shared_rows, _, _ = routed_rows(
+    spread = jnp.where(ids[None, :] == slots[:, 0:1], weights[:, 0:1], 0.0) + jnp.where(
+        ids[None, :] == slots[:, 1:2], weights[:, 1:2], 0.0
+    )
+    high = spread.astype(BF)
+    low = (spread - high.astype(F32)).astype(BF)
+    mixer_rows, expert_rows, _, _ = routed_rows(
         outbox,
         normed_b,
         (
@@ -744,22 +857,9 @@
             shared_up,
             shared_down,
         ),
+        jnp.concatenate([high, low], axis=1),
     )
-    returned = returned.reshape(slot_count, -1)
-    spread = jnp.where(ids[None, :] == slots[:, 0:1], weights[:, 0:1], 0.0) + jnp.where(
-        ids[None, :] == slots[:, 1:2], weights[:, 1:2], 0.0
-    )
-    high = spread.astype(BF)
-    low = (spread - high.astype(F32)).astype(BF)
-    combined = jnp.dot(high, returned, preferred_element_type=F32) + jnp.dot(
-        low, returned, preferred_element_type=F32
-    )
-    quarters = lax.all_to_all(
-        combined.astype(BF).reshape(tp_count, rows_own, -1), "tp", 0, 0, tiled=True
-    )
-    routed = jnp.moveaxis(quarters, 0, 1).reshape(rows_own, model_width)
-    experts_out = (shared_rows.astype(F32) + routed.astype(F32)).astype(BF)
-    return (mixer_rows, experts_out)
+    return (mixer_rows, expert_rows)
 
 
 def solution(mesh):

time: 270 us -> 251 us (0.930)
  Pallas kernels: 211 us -> 229 us
  waiting for transfers between devices: 15.5 us -> 0 us
  blocking collectives: 9.3 us -> 0 us
  matrix products: 15.4 us -> 7.75 us
  other arithmetic: 10 us -> 4.68 us
  local copies, waits for them, and re-layouts: 3.73 us -> 7.57 us
  starting transfers between devices: 3.52 us -> 0 us
    pallas_call x1 -> x2, Pallas kernels: 211 us -> 229 us  [the longest x1 222 us: routed_rows(): pl.pallas_call(expert_kernel, out_shape=(jax.ShapeDtypeStruct((block, wid...]
    all_to_all x1 -> x0, waiting for transfers between devices: 15.5 us -> none  [per_device(): lax.all_to_all(combined.astype(BF).reshape(tp_count, rows_own, -1), 'tp',...]
    all_gather x1 -> x0, blocking collectives: 9.3 us -> none  [per_device(): lax.all_gather(jnp.concatenate([routes.astype(F32), route_weights], axis=...]
    dot_general x3 -> x1, matrix products: 7.59 us -> 0.14 us  [per_device(): jnp.einsum('ij,bje->bie', lower, named, preferred_element_type=F32)]
    unnamed x26 -> x8, local copies, waits for them, and re-layouts: 1.2 us -> 7.48 us
    convert_element_type x5 -> x1, other arithmetic: 5.8 us -> 1.05 us  [per_device(): high = spread.astype(BF)]
    all_to_all x1 -> x0, starting transfers between devices: 3.52 us -> none  [per_device(): lax.all_to_all(combined.astype(BF).reshape(tp_count, rows_own, -1), 'tp',...]
    reduce_sum x1 -> x2, other arithmetic: 3.09 us -> 0.07 us  [the longest x1 0.05 us: per_device(): jnp.sum(jnp.where(onehot, earlier[:, :, None, :], 0.0), axis=3)]
  transfers between devices with their start and end apart: 1 -> 0, of which waited for: 1 -> 0; matrix products, arithmetic and copies ran while one was open for 0% -> 0% of each run, Pallas kernels for 0% -> 0%
where the time goes in v4:
time: 251 us; the launch traced here: 250 us
  Pallas kernels  229 us (91%)
  matrix products  7.75 us (3%)
  local copies, waits for them, and re-layouts  7.57 us (3%)
  other arithmetic  4.68 us (2%)
    pallas_call x1, Pallas kernels, routed_rows(): pl.pallas_call(expert_kernel, out_shape=(jax.ShapeDtypeStruct((block, wid...  222 us
    dot_general x1, matrix products, per_device(): outbox = jnp.dot(select, part, preferred_element_type=F32).astype(BF)  7.61 us
    unnamed x8, local copies, waits for them, and re-layouts  7.48 us
    pallas_call x1, Pallas kernels, normed_rows(): pl.pallas_call(norm_kernel, out_shape=(jax.ShapeDtypeStruct((4, *table.sh...  6.4 us

profile of v4, /device:TPU:1, one launch (start us, length us, event | category | flops | bytes accessed | tf_op | source)
XLA Modules:
  0.0 249.6 jit_solution(1225461735507983701)
XLA Ops:
  0.7 0.1 pad.4.clone
  0.7 0.7 convert_bitcast_fusion.1
  1.4 0.7 maximum_maximum_fusion.table
  2.2 0.0 copy-start.1
  2.2 2.2 copy-done.1
  4.4 0.0 copy-start.2
  4.4 0.7 copy-done.2
  5.1 6.4 %shard_map.176 = (f32[4,8,128]{2,1,0:T(8,128)S(1)}, bf16[512,4096]{1,0:T(8,128)(2,1)S(1)}) custom-call(f32[8,128]{1,0:T(8,128)S(1)} %maximum_maximum_fusion.table, bf16[512,4096]{1,0:T(8,128)(2,1)S(1)} %copy-done.1, f32[1,4096]{1,0:T(1,128)S(1)} %bitcast.31), custom_call_target="tpu_custom_call" | custom-call | tf_op jit(solution)/shard_map/pallas_call | solution.py:685
  11.5 0.0 copy-start
  11.5 0.1 convolution_bitcast_fusion
  11.7 0.1 select_reduce_fusion
  11.7 0.1 add_bitcast_fusion
  11.8 1.1 fusion
  12.9 2.0 pad_maximum_fusion.spread
  14.9 0.0 copy-done
  14.9 7.6 %convolution_convert_fusion = bf16[1536,3072]{1,0:T(8,128)(2,1)} fusion(bf16[512,4096]{1,0:T(8,128)(2,1)S(1)} %get-tuple-element.7.normed, s32[]{:T(128)S(6)} %select_n.23, s32[512]{0:T(512)S(1)} %bitcast.41, s32[512]{0:T(512)S(1)} %bitcast.39), kind=kOutput, calls=%fused_computation | convolution fusion | flops 4838916096 | bytes 12587012 | tf_op jit(solution)/shard_map/dot_general | solution.py:832
  22.5 222.5 %shard_map.177 = (bf16[128,4096]{1,0:T(8,128)(2,1)}, bf16[128,4096]{1,0:T(8,128)(2,1)}, bf16[9,2,48,3072]{3,2,1,0:T(8,128)(2,1)}, bf16[9,96,1024]{2,1,0:T(8,128)(2,1)}) custom-call(bf16[32,48,3072]{2,1,0:T(8,128)(2,1)} %bitcast.32, bf16[512,4096]{1,0:T(8,128)(2,1)} %copy-done, bf16[512,512]{1,0:T(8,128)(2,1)} %value_in.1, bf16[512,512]{1,0:T(8,128)(2,1)} %gate_in.1, ...), custom_call_target="tpu_custom_call" | custom-call | tf_op jit(solution)/shard_map/pallas_call | solution.py:711
  245.0 2.3 copy.25
  247.3 2.3 copy.26
  (6 shorter events, 0.0 us)
Async XLA Ops:
  2.2 2.2 copy-start.1
  4.4 0.7 copy-start.2
  11.5 3.5 %copy-start = (bf16[512,4096]{1,0:T(8,128)(2,1)}, bf16[512,4096]{1,0:T(8,128)(2,1)S(1)}, u32[]{:S(2)}) copy-start(bf16[512,4096]{1,0:T(8,128)(2,1)S(1)} %get-tuple-element.7.normed) | copy-start | bytes 12582916

commit v5 on v4

--- a/solution.py
+++ b/solution.py
@@ -411,11 +411,12 @@
     piece = block // 2
 
     def reduce_copy(n):
-        if n < 2:
-            source = part.at[across, :, pl.ds(n * wing, wing)]
-            target = first.at[n]
+        if n < 4:
+            span = pl.ds((n // 2) * block, block)
+            source = part.at[across, span, pl.ds(n % 2 * wing, wing)]
+            target = first.at[n % 2, span]
         else:
-            span = pl.ds((n // 2 - 1) * piece, piece)
+            span = pl.ds((n // 2 - 2) * piece, piece)
             source = part.at[right if n % 2 == 0 else left, span]
             target = second.at[n % 2, span]
         return pltpu.make_async_remote_copy(
@@ -427,14 +428,14 @@
             device_id_type=MESH,
         )
 
-    def reduce_start():
-        reduce_copy(0).start()
-        reduce_copy(1).start()
+    def reduce_start(which):
+        reduce_copy(2 * which).start()
+        reduce_copy(2 * which + 1).start()
 
     def reduce_pass(q):
-        if q == 0:
-            reduce_copy(0).wait_recv()
-            reduce_copy(1).wait_recv()
+        if q % 2 == 0:
+            reduce_copy(q).wait_recv()
+            reduce_copy(q + 1).wait_recv()
         span = pl.ds(q * piece, piece)
         for n, owner in ((0, right), (1, left)):
             for k in range(wing // 512):
@@ -443,10 +444,10 @@
                     part[owner, span, cols].astype(F32)
                     + first[n, span, 512 * k : 512 * k + 512].astype(F32)
                 ).astype(BF)
-            reduce_copy(2 * q + 2 + n).start()
+            reduce_copy(2 * q + 4 + n).start()
 
     def reduce_end():
-        for n in range(2, 10):
+        for n in range(4, 12):
             reduce_copy(n).wait_recv()
 
         def body(ks):
@@ -578,6 +579,7 @@
                 back_from_corner(2 * n + 1).start()
 
     shared_expert()
+    reduce_start(1)
     turn(range(0, 2))
     convolve()
     turn(range(2, 4))
@@ -587,7 +589,7 @@
     mix()
     load_spread.start()
     turn(range(6, 9))
-    reduce_start()
+    reduce_start(0)
     receive(1)
     loads[5].wait()
     loads[6].wait()
@@ -598,21 +600,21 @@
     own_weight.wait()
     for j in range(1, 4):
         weight_copy(j).wait()
-    reduce_pass(0)
     project(0)
     receive(3)
     pass_hidden(1)
     hidden(2)
-    reduce_pass(1)
+    reduce_pass(2)
     project(1)
     pass_hidden(2)
     hidden(3)
     turn_back(1)
     project(2)
     pass_hidden(3)
-    reduce_pass(2)
+    reduce_pass(3)
     project(3)
-    reduce_pass(3)
+    reduce_pass(0)
+    reduce_pass(1)
     turn_back(2)
     turn_back(3)
     own_back.wait()
@@ -626,7 +628,7 @@
     rim_copy.wait_send()
     for j in range(1, 4):
         stats_copy(j).wait_send()
-    for n in range(10):
+    for n in range(12):
         reduce_copy(n).wait_send()
     result[0].wait()
     for i in range(1, 32):
@@ -749,8 +751,8 @@
             dma((1,)),
             dma((4,)),
             dma((4,)),
-            dma((10,)),
-            dma((10,)),
+            dma((12,)),
+            dma((12,)),
             dma((32,)),
             dma((32,)),
             dma((32,)),

time: 251 us -> 236 us (0.940)
  Pallas kernels: 229 us -> 213 us
    pallas_call x1, Pallas kernels: 222 us -> 207 us  [routed_rows(): pl.pallas_call(expert_kernel, out_shape=(jax.ShapeDtypeStruct((block, wid...]
where the time goes in v5:
time: 236 us; the launch traced here: 234 us
  Pallas kernels  213 us (90%)
  matrix products  7.75 us (3%)
  local copies, waits for them, and re-layouts  7.57 us (3%)
  other arithmetic  4.68 us (2%)
    pallas_call x1, Pallas kernels, routed_rows(): pl.pallas_call(expert_kernel, out_shape=(jax.ShapeDtypeStruct((block, wid...  207 us
    dot_general x1, matrix products, per_device(): outbox = jnp.dot(select, part, preferred_element_type=F32).astype(BF)  7.61 us
    unnamed x8, local copies, waits for them, and re-layouts  7.48 us
    pallas_call x1, Pallas kernels, normed_rows(): pl.pallas_call(norm_kernel, out_shape=(jax.ShapeDtypeStruct((4, *table.sh...  6.4 us

profile of v5, /device:TPU:1, one launch (start us, length us, event | category | flops | bytes accessed | tf_op | source)
XLA Modules:
  0.0 233.7 jit_solution(11832500571636149542)
XLA Ops:
  0.7 0.1 pad.4.clone
  0.7 0.7 convert_bitcast_fusion.1
  1.4 0.7 maximum_maximum_fusion.table
  2.2 0.0 copy-start.1
  2.2 2.2 copy-done.1
  4.4 0.0 copy-start.2
  4.4 0.7 copy-done.2
  5.1 6.4 %shard_map.176 = (f32[4,8,128]{2,1,0:T(8,128)S(1)}, bf16[512,4096]{1,0:T(8,128)(2,1)S(1)}) custom-call(f32[8,128]{1,0:T(8,128)S(1)} %maximum_maximum_fusion.table, bf16[512,4096]{1,0:T(8,128)(2,1)S(1)} %copy-done.1, f32[1,4096]{1,0:T(1,128)S(1)} %bitcast.31), custom_call_target="tpu_custom_call" | custom-call | tf_op jit(solution)/shard_map/pallas_call | solution.py:687
  11.5 0.0 copy-start
  11.5 0.1 convolution_bitcast_fusion
  11.7 0.1 select_reduce_fusion
  11.7 0.1 add_bitcast_fusion
  11.8 1.1 fusion
  12.9 2.0 pad_maximum_fusion.spread
  14.9 0.0 copy-done
  14.9 7.6 %convolution_convert_fusion = bf16[1536,3072]{1,0:T(8,128)(2,1)} fusion(bf16[512,4096]{1,0:T(8,128)(2,1)S(1)} %get-tuple-element.7.normed, s32[]{:T(128)S(6)} %select_n.23, s32[512]{0:T(512)S(1)} %bitcast.41, s32[512]{0:T(512)S(1)} %bitcast.39), kind=kOutput, calls=%fused_computation | convolution fusion | flops 4838916096 | bytes 12587012 | tf_op jit(solution)/shard_map/dot_general | solution.py:834
  22.5 206.6 %shard_map.177 = (bf16[128,4096]{1,0:T(8,128)(2,1)}, bf16[128,4096]{1,0:T(8,128)(2,1)}, bf16[9,2,48,3072]{3,2,1,0:T(8,128)(2,1)}, bf16[9,96,1024]{2,1,0:T(8,128)(2,1)}) custom-call(bf16[32,48,3072]{2,1,0:T(8,128)(2,1)} %bitcast.32, bf16[512,4096]{1,0:T(8,128)(2,1)} %copy-done, bf16[512,512]{1,0:T(8,128)(2,1)} %value_in.1, bf16[512,512]{1,0:T(8,128)(2,1)} %gate_in.1, ...), custom_call_target="tpu_custom_call" | custom-call | tf_op jit(solution)/shard_map/pallas_call | solution.py:713
  229.1 2.3 copy.25
  231.4 2.3 copy.26
  (6 shorter events, 0.0 us)
Async XLA Ops:
  2.2 2.2 copy-start.1
  4.4 0.7 copy-start.2
  11.5 3.5 %copy-start = (bf16[512,4096]{1,0:T(8,128)(2,1)}, bf16[512,4096]{1,0:T(8,128)(2,1)S(1)}, u32[]{:S(2)}) copy-start(bf16[512,4096]{1,0:T(8,128)(2,1)S(1)} %get-tuple-element.7.normed) | copy-start | bytes 12582916
